TPU v7x, 32 devices: a whole 2x2x4 slice. The times are simulated.
32 devices in a mesh: ep: 8 (over z, y), tp: 4 (over x, core).
Axes of the slice: x: 2, y: 2, z: 4, core: 2. Of those that a mesh axis runs over, the one named last changes fastest.
Arguments:
- query_rows: bfloat16 [4096, 1024], P('ep', 'tp'), may hold values from -10 to 10
- key_rows: bfloat16 [4096, 1024], P('ep', 'tp'), may hold values from -10 to 10
- value_rows: bfloat16 [4096, 1024], P('ep', 'tp'), may hold values from -6 to 6
- key_bias: float32 [4096, 16], P(None, 'tp'), may hold values from -30 to 0
- out_weight: bfloat16 [1024, 2048], P('tp'), may hold values from -0.5625 to 0.5625
- moe_input: bfloat16 [4096, 2048], P(('ep', 'tp')), may hold values from -6 to 6
- moe_gain: float32 [2048], replicated, may hold values from 0.1 to 1.9
- expert_pick: int32 [4096, 2], P(('ep', 'tp')), may hold values from 0 to 7, as said below
- route_weight: float32 [4096, 2], P(('ep', 'tp')), may hold values from 0.1 to 1
- w_gate: bfloat16 [8, 2048, 1024], P('ep', None, 'tp'), may hold values from -0.125 to 0.125
- w_up: bfloat16 [8, 2048, 1024], P('ep', None, 'tp'), may hold values from -0.125 to 0.125
- w_down: bfloat16 [8, 1024, 2048], P('ep', 'tp'), may hold values from -0.1875 to 0.1875
Outputs:
- mixer_out: bfloat16 [4096, 2048], P(('ep', 'tp'))
- routed_out: bfloat16 [4096, 2048], P(('ep', 'tp'))
Inputs may be any that keep to these rules, and one draw needn't show every extreme that they name: `expert_pick`: each row names two different experts of one group, expert e belonging to group e // 2; the rows of one device name no expert more than 64 times, and in every draw each expert of some group is named exactly 64 times by the rows of every device.
All inputs are finite; a program needn't handle non-finite values.
Results may differ from a plain program's by a relative error of at most 0.013.
Values may be sent and summed in bfloat16 or wider, within the bound.
No kernel may reach another device: no remote copies, remote signals or barrier semaphores. Data moves between devices by JAX's collectives and lax.ppermute only.
A program may use at most 128 MiB of HBM per device.

v0:
```python
import jax
import jax.numpy as jnp
from jax import lax
from jax.sharding import PartitionSpec as P

HEAD_DIM = 64
GROUPS = 4
TOPK = 2
SEQS = 1


norm_eps = 1e-06


def block_scores(query_grid, query_pos, key_block, bias_block, key_first):
    key_count = key_block.shape[0]
    head_count = query_grid.shape[1]
    head_width = query_grid.shape[2]
    key_grid = key_block.reshape(key_count, head_count, head_width)
    scores = jnp.einsum("qhd,khd->hqk", query_grid, key_grid, preferred_element_type=jnp.float32)
    scores = scores * head_width ** (-0.5) + jnp.transpose(bias_block)[:, None, :]
    key_pos = key_first + jnp.arange(key_count, dtype=jnp.int32)
    causal = (key_pos[None, :] < query_pos[:, None])[None]
    failure = jnp.where(causal, jax.nn.log_sigmoid(-scores), 0.0)
    return (scores, causal, failure)


def block_values(query_grid, query_pos, key_block, value_block, bias_block, key_first, running):
    scores, causal, failure = block_scores(query_grid, query_pos, key_block, bias_block, key_first)
    remainder = lax.cumsum(failure, axis=2, reverse=True) - failure + running[:, :, None]
    stick_weight = jnp.where(causal, jnp.exp(jax.nn.log_sigmoid(scores) + remainder), 0.0).astype(
        jnp.bfloat16
    )
    value_grid = value_block.reshape(value_block.shape[0], query_grid.shape[1], query_grid.shape[2])
    portion = jnp.einsum(
        "hqk,khd->hqd", stick_weight, value_grid, preferred_element_type=jnp.float32
    )
    return (portion, running + jnp.sum(failure, axis=2))


def held_attend(
    query_grid, query_pos, top_block, seq_base, all_keys, all_values, key_bias, block_rows
):
    row_count = query_grid.shape[0]
    head_count = query_grid.shape[1]
    zero_sum = jnp.zeros((head_count, row_count, query_grid.shape[2]), jnp.float32)
    zero_run = jnp.zeros((head_count, row_count), jnp.float32)

    def visit(step_index, carried):
        key_first = (top_block - step_index) * block_rows
        portion, running = block_values(
            query_grid,
            query_pos,
            lax.dynamic_slice_in_dim(all_keys, key_first, block_rows, 0),
            lax.dynamic_slice_in_dim(all_values, key_first, block_rows, 0),
            lax.dynamic_slice_in_dim(key_bias, key_first, block_rows, 0),
            key_first,
            carried[1],
        )
        return (carried[0] + portion, running)

    return lax.fori_loop(0, top_block - seq_base + 1, visit, (zero_sum, zero_run))[0]


def expand(arrived, gate_weights, up_weights):
    gate_in = jnp.einsum(
        "necm,emf->necf", arrived, gate_weights, preferred_element_type=jnp.float32
    )
    up_in = jnp.einsum("necm,emf->necf", arrived, up_weights, preferred_element_type=jnp.float32)
    return (jax.nn.silu(gate_in) * up_in).astype(jnp.bfloat16)


def contract(hidden, down_weights):
    return jnp.einsum("necf,efm->necm", hidden, down_weights, preferred_element_type=jnp.float32)


def local(
    query_rows,
    key_rows,
    value_rows,
    key_bias,
    out_weight,
    moe_input,
    moe_gain,
    expert_pick,
    route_weight,
    w_gate,
    w_up,
    w_down,
):
    block_rows = query_rows.shape[0]
    half_rows = block_rows // 2
    local_heads = query_rows.shape[1] // HEAD_DIM
    ep_index = lax.axis_index("ep")
    ep_count = lax.axis_size("ep")
    seq_blocks = ep_count // SEQS
    seq_base = ep_index // seq_blocks * seq_blocks
    first_pos = ep_index * block_rows + jnp.arange(half_rows, dtype=jnp.int32)
    second_pos = ep_index * block_rows + half_rows + jnp.arange(half_rows, dtype=jnp.int32)
    query_pos = jnp.concatenate([first_pos, second_pos], axis=0)
    query_grid = query_rows.reshape(block_rows, local_heads, HEAD_DIM)
    all_keys, all_values = (
        lax.all_gather(key_rows, "ep", axis=0, tiled=True),
        lax.all_gather(value_rows, "ep", axis=0, tiled=True),
    )
    attended_sum = held_attend(
        query_grid, query_pos, ep_index, seq_base, all_keys, all_values, key_bias, block_rows
    )
    attended = attended_sum.astype(jnp.bfloat16)
    out_heads = out_weight.reshape(local_heads, HEAD_DIM, out_weight.shape[1])
    chosen = attended
    mixer_out = lax.psum_scatter(
        jnp.einsum("hqd,hdm->qm", chosen, out_heads, preferred_element_type=jnp.float32).astype(
            jnp.bfloat16
        ),
        "tp",
        scatter_dimension=0,
        tiled=True,
    )
    token_count = moe_input.shape[0]
    widened = moe_input.astype(jnp.float32)
    normed = (
        widened
        * lax.rsqrt(jnp.mean(widened * widened, axis=1, keepdims=True) + norm_eps)
        * moe_gain
    ).astype(jnp.bfloat16)
    local_experts = w_gate.shape[0]
    expert_total = local_experts * ep_count
    capacity = GROUPS * token_count // expert_total
    picks = expert_pick.reshape(-1)
    matches = (picks[:, None] == jnp.arange(expert_total, dtype=jnp.int32)[None, :]).astype(
        jnp.int32
    )
    ranks = jnp.sum((jnp.cumsum(matches, axis=0) - matches) * matches, axis=1)
    slots = picks * capacity + ranks
    owners = jnp.arange(picks.shape[0], dtype=jnp.int32) // TOPK
    table = jnp.full((expert_total * capacity,), token_count, jnp.int32).at[slots].set(owners)
    padded = jnp.concatenate([normed, jnp.zeros((1, normed.shape[1]), jnp.bfloat16)], axis=0)
    outgoing = padded[table].reshape(ep_count, local_experts, capacity, normed.shape[1])
    arrived = lax.all_to_all(outgoing, "ep", split_axis=0, concat_axis=0, tiled=True)
    gate_all, up_all, down_all = (
        lax.all_gather(w_gate, "tp", axis=2, tiled=True),
        lax.all_gather(w_up, "tp", axis=2, tiled=True),
        lax.all_gather(w_down, "tp", axis=1, tiled=True),
    )
    served = contract(expand(arrived, gate_all, up_all), down_all).astype(jnp.bfloat16)
    returned = lax.all_to_all(served, "ep", split_axis=0, concat_axis=0, tiled=True)
    flat = returned.reshape(expert_total * capacity, returned.shape[3])
    chosen = flat[slots].reshape(token_count, TOPK, flat.shape[1]).astype(jnp.float32)
    routed_out = jnp.sum(chosen * route_weight[:, :, None], axis=1).astype(jnp.bfloat16)
    return (mixer_out, routed_out)


def solution(mesh):
    placed = (
        P("ep", "tp"),
        P("ep", "tp"),
        P("ep", "tp"),
        P(None, "tp"),
        P("tp", None),
        P(("ep", "tp"), None),
        P(),
        P(("ep", "tp"), None),
        P(("ep", "tp"), None),
        P("ep", None, "tp"),
        P("ep", None, "tp"),
        P("ep", "tp", None),
    )
    return jax.shard_map(
        local,
        mesh=mesh,
        in_specs=placed,
        out_specs=(P(("ep", "tp"), None), P(("ep", "tp"), None)),
        check_vma=False,
    )
```

profile of v0, /device:TPU:0, one launch (start us, length us, event | category | flops | bytes accessed | tf_op | source)
XLA Modules:
  0.0 587.7 jit_solution(13059920495421676207)
XLA Ops:
  7.2 1.9 copy.34
  9.2 1.8 copy.36
  15.8 1.4 scatter_custom_fusion
  17.2 3.3 gather_fusion
  20.5 7.4 %all-to-all-start = ((bf16[8,1,64,2048]{3,2,1,0:T(8,128)(2,1)}), bf16[8,1,64,2048]{3,2,1,0:T(8,128)(2,1)}, u32[]{:S(2)}, u32[]{:S(2)}) async-start(bf16[8,1,64,2048]{3,2,1,0:T(8,128)(2,1)} %bitcast.165), calls=%async_computation.1 | async-start | bytes 4194304 | tf_op jit(solution)/shard_map/all_to_all | solution.py:140
  28.8 67.5 %all-gather.6.cloned.1.call-done = bf16[4096,256]{0,1:T(8,128)(2,1)} async-done(((bf16[512,256]{0,1:T(8,128)(2,1)}), bf16[4096,256]{0,1:T(8,128)(2,1)}) %all-gather.6.cloned.1.call-update) | async-done | bytes 2097168 | tf_op jit(solution)/shard_map/all_gather | solution.py:103
  96.3 52.0 %all-gather.8.cloned.1.call-done = bf16[4096,256]{0,1:T(8,128)(2,1)} async-done(((bf16[512,256]{0,1:T(8,128)(2,1)}), bf16[4096,256]{0,1:T(8,128)(2,1)}) %all-gather.8.cloned.1.call-update) | async-done | bytes 2097168 | tf_op jit(solution)/shard_map/all_gather | solution.py:104
  148.4 67.8 %while.12 = (s32[]{:T(128)}, f32[4,512,64]{1,2,0:T(8,128)S(1)}, f32[4,512]{1,0:T(4,128)S(1)}, s32[]{:T(128)}, s32[]{:T(128)}, /*index=5*/s32[512]{0:T(512)S(1)},...) while((s32[]{:T(128)}, f32[4,512,64]{1,2,0:T(8,128)S(1)}, ...), condition=%wide.region_4.5_spmd, body=%wide.region_0.4_spmd.sunk | while | flops 438729216 | bytes 83679512 | solution.py:62
  167.6 1.1 constant_dynamic-slice_fusion.3
  169.6 5.1 fusion.74
  174.7 19.4 %fusion.75 = f32[4,512,4,128]{1,2,3,0:T(4,128)S(1)} fusion(f32[4,512,4,128]{1,3,2,0:T(8,128)S(1)} %bitcast.162), kind=kOutput, calls=%fused_computation.21.clone.1 | output fusion | flops 133169152 | bytes 8388608 | tf_op jit(solution)/shard_map/reduce-window
  194.0 1.9 copy-done.1
  196.1 2.9 broadcast_add_fusion.2
  199.0 1.3 copy.49
  201.2 6.7 %fusion.76 = bf16[4,512,512]{1,2,0:T(8,128)(2,1)S(1)} fusion(f32[4,512,4,128]{1,3,2,0:T(8,128)S(1)} %copy.49, f32[4,512,512]{2,1,0:T(8,128)S(1)} %copy-done.2, f32[4,512]{1,0:T(4,128)S(1)} %get-tuple-element.172, f32[4,512]{1,0:T(4,128)S(1)} %dynamic-slice_bitcast_fusion.2, pred[512,512]{0,1:T(8,128)(4,1)S(1)} %broadcast_compare_fusion.2), kind=kLoop, calls=%fused_computation.9.clone.1 | loop fusion | flops 24117248 | bytes 10764288 | tf_op jit(solution)/shard_map/while/body/convert_element_type | solution.py:31
  216.2 2.1 bitcast_convert_fusion
  218.4 5.2 fusion.17
  223.6 31.9 %all-gather.10.cloned.1.call-done = bf16[1,2048,1024]{2,1,0:T(8,128)(2,1)} async-done(((bf16[1,2048,256]{2,1,0:T(8,128)(2,1)}), bf16[1,2048,1024]{2,1,0:T(8,128)(2,1)}) %all-gather.10.cloned.1.call-update) | async-done | bytes 4194320 | tf_op jit(solution)/shard_map/all_gather | solution.py:142
  255.4 10.2 %fusion.24 = bf16[8,1,64,2048]{3,2,1,0:T(8,128)(2,1)} fusion(bf16[1,1024,2048]{2,1,0:T(8,128)(2,1)} %all-gather.14.cloned.1.call-done, f32[8,64,1024]{2,1,0:T(8,128)S(1)} %fusion.17, bf16[1,2048,1024]{2,1,0:T(8,128)(2,1)} %all-gather.10.cloned.1.call-done, bf16[8,1,64,2048]{3,2,1,0:T(8,128)(2,1)} %all-to-all-done), kind=kOutput, calls=%fused_computation.41 | convolution fusion | flops 4299161600 | bytes 14680064 | tf_op jit(solution)/shard_map/necf,efm->necm/dot_general | solution.py:74
  265.6 258.2 %all-to-all-start.1 = ((bf16[8,1,64,2048]{3,2,1,0:T(8,128)(2,1)}), bf16[8,1,64,2048]{3,2,1,0:T(8,128)(2,1)S(1)}, u32[]{:S(2)}, u32[]{:S(2)}) async-start(bf16[8,1,64,2048]{3,2,1,0:T(8,128)(2,1)} %fusion.24), calls=%async_computation.2 | async-start | bytes 4194304 | tf_op jit(solution)/shard_map/all_to_all | solution.py:147
  523.9 48.2 %all-to-all-done.1 = bf16[8,1,64,2048]{3,2,1,0:T(8,128)(2,1)S(1)} async-done(((bf16[8,1,64,2048]{3,2,1,0:T(8,128)(2,1)}), bf16[8,1,64,2048]{3,2,1,0:T(8,128)(2,1)S(1)}, u32[]{:S(2)}, u32[]{:S(2)}) %all-to-all-start.1) | async-done | bytes 2097184 | tf_op jit(solution)/shard_map/all_to_all | solution.py:147
  572.1 2.3 gather_fusion.1
  574.4 2.4 reshape.153
  576.8 3.9 multiply_reduce_fusion
  (64 shorter events, 8.2 us)
Async XLA Ops:
  7.2 209.1 %copy-start = (bf16[256,2048]{1,0:T(8,128)(2,1)S(1)}, bf16[256,2048]{1,0:T(8,128)(2,1)}, u32[]{:S(2)}) copy-start(bf16[256,2048]{1,0:T(8,128)(2,1)} %param.18) | copy-start | bytes 3145732
  7.2 8.1 %copy-start.3 = (bf16[128,2048]{1,0:T(8,128)(2,1)S(1)}, bf16[128,2048]{1,0:T(8,128)(2,1)}, u32[]{:S(2)}) copy-start(bf16[128,2048]{1,0:T(8,128)(2,1)} %param.19) | copy-start | bytes 1572868
  7.2 8.2 %copy-start.5 = (f32[2048]{0:T(1024)S(1)}, f32[2048]{0:T(1024)}, u32[]{:S(2)}) copy-start(f32[2048]{0:T(1024)} %param.20) | copy-start | bytes 24580
  7.2 89.1 %all-gather.6.cloned.1.call-start = ((), (), s32[]{:S(2)}) async-start(), calls=%async_computation.3 | async-start | bytes 2359296 | tf_op jit(solution)/shard_map/all_gather | solution.py:103
  9.2 139.1 %all-gather.8.cloned.1.call-start = ((), (), s32[]{:S(2)}) async-start(), calls=%async_computation.4 | async-start | bytes 2359296 | tf_op jit(solution)/shard_map/all_gather | solution.py:104
  11.0 207.3 %all-gather.12.cloned.1.call-start = ((), (), s32[]{:S(2)}) async-start(), calls=%async_computation.7 | async-start | bytes 5242880 | tf_op jit(solution)/shard_map/all_gather | solution.py:143
  11.8 211.8 %all-gather.14.cloned.1.call-start = ((), (), s32[]{:S(2)}) async-start(), calls=%async_computation.8 | async-start | bytes 5242880 | tf_op jit(solution)/shard_map/all_gather | solution.py:144
  20.5 8.1 %copy-start.4 = (bf16[512,256]{1,0:T(8,128)(2,1)S(1)}, bf16[512,256]{1,0:T(8,128)(2,1)}, u32[]{:S(2)}) copy-start(bf16[512,256]{1,0:T(8,128)(2,1)} %param.14) | copy-start | bytes 786436
  20.5 197.8 %all-to-all-start = ((bf16[8,1,64,2048]{3,2,1,0:T(8,128)(2,1)}), bf16[8,1,64,2048]{3,2,1,0:T(8,128)(2,1)}, u32[]{:S(2)}, u32[]{:S(2)}) async-start(bf16[8,1,64,2048]{3,2,1,0:T(8,128)(2,1)} %bitcast.165), calls=%async_computation.1 | async-start | bytes 4194304 | tf_op jit(solution)/shard_map/all_to_all | solution.py:140
  28.0 227.5 %all-gather.10.cloned.1.call-start = ((), (), s32[]{:S(2)}) async-start(), calls=%async_computation.6 | async-start | bytes 5242880 | tf_op jit(solution)/shard_map/all_gather | solution.py:142
  28.6 552.1 %reduce-scatter.2.cloned.1.call-start = ((), (), s32[]{:S(2)}) async-start(), calls=%async_computation.5 | async-start | bytes 2621440 | tf_op jit(solution)/shard_map/reduce_scatter | solution.py:112
  194.0 1.9 copy-start.1
  199.0 2.2 copy-start.2
  265.6 258.2 %copy-start.6 = (f32[128,2]{0,1:T(2,128)S(1)}, f32[128,2]{0,1:T(2,128)}, u32[]{:S(2)}) copy-start(f32[128,2]{0,1:T(2,128)} %param.22) | copy-start | bytes 3076
  265.6 306.5 %all-to-all-start.1 = ((bf16[8,1,64,2048]{3,2,1,0:T(8,128)(2,1)}), bf16[8,1,64,2048]{3,2,1,0:T(8,128)(2,1)S(1)}, u32[]{:S(2)}, u32[]{:S(2)}) async-start(bf16[8,1,64,2048]{3,2,1,0:T(8,128)(2,1)} %fusion.24), calls=%async_computation.2 | async-start | bytes 4194304 | tf_op jit(solution)/shard_map/all_to_all | solution.py:147
Sparse Core Ops, SparseCore 0:
  10.6 85.6 all-gather.5
  98.9 49.3 all-gather.7
  149.9 33.1 all-gather.11
  184.5 34.4 all-gather.13
  220.4 34.9 all-gather.9
  258.4 275.6 reduce-scatter.1
where the time goes:
time: 593 us; the launch traced here: 588 us
  starting transfers between devices  266 us (45%)
  waiting for transfers between devices  201 us (34%)
  other arithmetic  35 us (6%)
  loops' own time  27.1 us (5%)
  matrix products  23 us (4%)
  local copies, waits for them, and re-layouts  20.9 us (4%)
  between operations  14.5 us (2%)
    all_to_all x1, starting transfers between devices, local(): lax.all_to_all(served, 'ep', split_axis=0, concat_axis=0, tiled=True)  258 us
    all_gather x1, waiting for transfers between devices, local(): lax.all_gather(key_rows, 'ep', axis=0, tiled=True)  67.5 us
    all_gather x1, waiting for transfers between devices, local(): lax.all_gather(value_rows, 'ep', axis=0, tiled=True)  52 us
    all_to_all x1, waiting for transfers between devices, local(): lax.all_to_all(served, 'ep', split_axis=0, concat_axis=0, tiled=True)  48.2 us
    all_gather x1, waiting for transfers between devices, local(): lax.all_gather(w_gate, 'tp', axis=2, tiled=True)  31.9 us
    another operation x1, loops' own time, held_attend(): lax.fori_loop(0, top_block - seq_base + 1, visit, (zero_sum, zero_run))[0]  27.1 us
    another operation x4, other arithmetic  20.1 us
  transfers between devices with their start and end apart: 8, of which 4 were waited for; matrix products, arithmetic and copies ran while one was open for 13% of the time, Pallas kernels for 0%

commit v1 on v0

v1 whole, which is shorter than its diff:
```python
import functools
import math

import jax
import jax.numpy as jnp
from jax import lax
from jax.experimental import pallas as pl
from jax.experimental.pallas import tpu as pltpu
from jax.sharding import PartitionSpec as P

HEAD_DIM = 64
GROUPS = 4
TOPK = 2
LANES = 128
KEY_TILE = 256
LOG2E = math.log2(math.e)
MIB = 1 << 20

norm_eps = 1e-06
bf16 = jnp.bfloat16
f32 = jnp.float32

VMEM = pl.BlockSpec(memory_space=pltpu.VMEM)
SMEM = pl.BlockSpec(memory_space=pltpu.SMEM)


def call(body, name, outs, ins, limit, flops=0, moved=0):
    return pl.pallas_call(
        body,
        name=name,
        out_shape=outs,
        in_specs=ins,
        out_specs=jax.tree.map(lambda _: VMEM, outs),
        compiler_params=pltpu.CompilerParams(vmem_limit_bytes=limit * MIB),
        cost_estimate=pl.CostEstimate(flops=flops, bytes_accessed=moved, transcendentals=0),
    )


def mm(a, b):
    return jnp.dot(a, b, preferred_element_type=f32)


def pack_body(q_ref, k_ref, v_ref, out_ref, *, heads, sharers, parts):
    rows = q_ref.shape[0]
    part_rows = rows // parts
    sub = part_rows // sharers
    half = rows // sharers // 2
    for h in range(heads):
        cols = pl.ds(h * HEAD_DIM, HEAD_DIM)
        pair = jnp.concatenate([k_ref[:, cols], v_ref[:, cols]], axis=1)
        for s in range(sharers):
            out_ref[h * sharers + s, :rows] = pair
            mine = jnp.concatenate(
                [q_ref[pl.ds(t * part_rows + s * sub, sub), cols] for t in range(parts)], axis=0
            )
            out_ref[h * sharers + s, rows:] = jnp.concatenate([mine[:half], mine[half:]], axis=1)


def attend_body(where_ref, got_ref, bias_ref, out_ref, *, rows, sub, parts):
    blocks = got_ref.shape[0]
    mine = sub * parts
    half = mine // 2
    share = where_ref[0]
    scale = HEAD_DIM**-0.5 * LOG2E
    tiles = rows // KEY_TILE
    part_rows = rows // parts
    low = lax.broadcasted_iota(jnp.int32, (half, LANES), 1) < HEAD_DIM
    later = (
        lax.broadcasted_iota(jnp.int32, (KEY_TILE, KEY_TILE), 0)
        > lax.broadcasted_iota(jnp.int32, (KEY_TILE, KEY_TILE), 1)
    )
    after = jnp.where(later, 1.0, 0.0).astype(bf16)
    row = lax.broadcasted_iota(jnp.int32, (mine, KEY_TILE), 0)
    spot = row + share * sub
    for t in range(1, parts):
        spot = spot + jnp.where(row >= t * sub, part_rows - sub, 0)
    lane = lax.broadcasted_iota(jnp.int32, (mine, KEY_TILE), 1)

    def tile(query, source, c, masked):
        pair = got_ref[source, pl.ds(c * KEY_TILE, KEY_TILE)]
        bias = bias_ref[pl.ds(source * tiles + c, 1)]
        raw = lax.dot_general(query, pair, (((1,), (1,)), ((), ())), preferred_element_type=f32)
        score = raw * scale + bias
        soft = jnp.maximum(score, 0.0) + jnp.log2(1.0 + jnp.exp2(-jnp.abs(score)))
        if masked:
            causal = lane + c * KEY_TILE < spot
            soft = jnp.where(causal, soft, 0.0)
        rounded = soft.astype(bf16)
        rest = mm(rounded, after)
        weight = jnp.exp2(score - soft - rest)
        if masked:
            weight = jnp.where(causal, weight, 0.0)
        total = rest[:, :1] + rounded[:, :1].astype(f32)
        return mm(weight.astype(bf16), pair), total

    def visit(query, source, state, masked):
        found = [tile(query, source, c, masked) for c in reversed(range(tiles))]
        acc, carry = state
        for portion, total in found:
            acc = acc + portion * jnp.exp2(-carry)
            carry = carry + total
        return acc, carry

    def one_block(b, _):
        packed = got_ref[b, pl.ds(rows, half)].astype(f32)
        query = jnp.concatenate(
            [
                jnp.where(low, packed, 0.0),
                jnp.where(low, pltpu.roll(packed, HEAD_DIM, 1), 0.0),
            ],
            axis=0,
        ).astype(bf16)
        state = (jnp.zeros((mine, LANES), f32), jnp.zeros((mine, 1), f32))
        state = visit(query, b, state, True)
        acc, _ = lax.fori_loop(
            0, b, lambda i, st: visit(query, b - 1 - i, st, False), state
        )
        turned = pltpu.roll(acc, HEAD_DIM, 1)
        few = sub // 2
        keep = lax.broadcasted_iota(jnp.int32, (few, LANES), 1) < HEAD_DIM
        for t in range(parts):
            first = turned[t * sub : t * sub + few]
            second = acc[t * sub + few : (t + 1) * sub]
            out_ref[b, t] = jnp.where(keep, first, second).astype(bf16)
        return 0

    lax.fori_loop(0, blocks, one_block, 0)


def project_body(where_ref, got_ref, w0, w1, w2, w3, out_ref, *, heads, sharers, parts):
    here = where_ref[1]
    few = got_ref.shape[1]
    low = lax.broadcasted_iota(jnp.int32, (few, LANES), 1) < HEAD_DIM
    total = None
    for m, w_ref in enumerate((w0, w1, w2, w3)):
        tp = here ^ m
        strips = []
        for s in range(sharers):
            firsts, seconds = [], []
            for h in range(0, heads, 2):
                a = got_ref[(h * sharers + s) * parts + tp].astype(f32)
                b = got_ref[((h + 1) * sharers + s) * parts + tp].astype(f32)
                firsts.append(jnp.where(low, a, pltpu.roll(b, HEAD_DIM, 1)))
                seconds.append(jnp.where(low, pltpu.roll(a, HEAD_DIM, 1), b))
            strips.append(jnp.concatenate(firsts, axis=1))
            strips.append(jnp.concatenate(seconds, axis=1))
        left = jnp.concatenate(strips, axis=0).astype(bf16)
        part = mm(left, w_ref[...])
        total = part if total is None else total + part
    out_ref[...] = total.astype(bf16)


def spread(piece, size):
    cross = [(i, i ^ 2) for i in range(size)]
    beside = [(i, i ^ 1) for i in range(size)]
    far = lax.ppermute(piece, "tp", cross)
    near = lax.ppermute(piece, "tp", beside)
    return (piece, near, far, lax.ppermute(far, "tp", beside))


def mixer(query_rows, key_rows, value_rows, key_bias, out_pieces):
    rows = query_rows.shape[0]
    heads = query_rows.shape[1] // HEAD_DIM
    ep_count = lax.axis_size("ep")
    parts = lax.axis_size("tp")
    ep_index = lax.axis_index("ep")
    tp_index = lax.axis_index("tp")
    sharers = ep_count // heads
    sub = rows // parts // sharers
    mine = sub * parts
    tall = rows + mine // 2
    outgoing = call(
        functools.partial(pack_body, heads=heads, sharers=sharers, parts=parts),
        "pack",
        jax.ShapeDtypeStruct((ep_count, tall, LANES), bf16),
        [VMEM] * 3,
        32,
    )(query_rows, key_rows, value_rows)
    got = lax.all_to_all(outgoing, "ep", split_axis=0, concat_axis=0, tiled=True)
    head = ep_index // sharers
    bias = lax.dynamic_index_in_dim(key_bias, head, 1, keepdims=False) * LOG2E
    bias = bias.reshape(-1, KEY_TILE)
    where = jnp.stack([ep_index % sharers, tp_index]).astype(jnp.int32)
    attended = call(
        functools.partial(attend_body, rows=rows, sub=sub, parts=parts),
        "attend",
        jax.ShapeDtypeStruct((ep_count, parts, sub // 2, LANES), bf16),
        [SMEM, VMEM, VMEM],
        48,
        flops=3 * ep_count * ep_count * mine * rows * LANES,
    )(where, got, bias)
    attended = attended.reshape(ep_count * parts, sub // 2, LANES)
    back = lax.all_to_all(attended, ("ep", "tp"), split_axis=0, concat_axis=0, tiled=True)
    return call(
        functools.partial(project_body, heads=heads, sharers=sharers, parts=parts),
        "project",
        jax.ShapeDtypeStruct((rows // parts, out_pieces[0].shape[1]), bf16),
        [SMEM] + [VMEM] * 5,
        48,
        flops=2 * rows * heads * HEAD_DIM * out_pieces[0].shape[1],
    )(where, back, *out_pieces)


def route_body(zy_ref, x_ref, gain_ref, pick_t_ref, pick_ref, weight_ref, *outs, cap):
    out_refs, turn_ref = outs[:-1], outs[-1]
    tokens, width = x_ref.shape
    wide = x_ref[...].astype(f32)
    normed = (
        wide
        * lax.rsqrt(jnp.mean(wide * wide, axis=1, keepdims=True) + norm_eps)
        * gain_ref[...]
    ).astype(bf16)
    z = zy_ref[0]
    pick = pick_t_ref[0:1, :]
    lanes = GROUPS * 2
    group = lax.broadcasted_iota(jnp.int32, (lanes, tokens), 0)
    inside = (pick >= group * TOPK) & (pick < (group + 1) * TOPK)
    match = jnp.where(inside, 1.0, 0.0)
    before = (
        lax.broadcasted_iota(jnp.int32, (tokens, tokens), 0)
        < lax.broadcasted_iota(jnp.int32, (tokens, tokens), 1)
    )
    rank = mm(match.astype(bf16), jnp.where(before, 1.0, 0.0).astype(bf16))
    first = ((group ^ z) * cap).astype(f32)
    slot = jnp.sum(match * (rank + first), axis=0, keepdims=True).astype(jnp.int32)
    place = lax.broadcasted_iota(jnp.int32, (GROUPS * cap, tokens), 0) == slot
    place = jnp.where(place, 1.0, 0.0)
    weight = weight_ref[...]
    odd = (pick_ref[...] & 1) == 1
    one = jnp.sum(jnp.where(odd, weight, 0.0), axis=1, keepdims=True)
    zero = jnp.sum(jnp.where(odd, 0.0, weight), axis=1, keepdims=True)
    lane = lax.broadcasted_iota(jnp.int32, (tokens, LANES), 1)
    value = jnp.where((lane & 1) == 1, one, zero)
    high = value.astype(bf16).astype(f32)
    extra = jnp.where(lane < 2, high, value - high).astype(bf16)
    place_b = place.astype(bf16)
    for k, ref in enumerate(out_refs):
        strip = place_b[k * cap : (k + 1) * cap]
        ref[:, :width] = mm(strip, normed).astype(bf16)
        ref[:, width:] = mm(strip, extra).astype(bf16)
    turn_ref[...] = place.T.astype(bf16)


def expand_body(*refs):
    rows, gates, ups, out_ref = refs[:8], refs[8:12], refs[12:16], refs[16]
    width = gates[0].shape[0]
    cap = rows[0].shape[0]
    part = gates[0].shape[1]
    x = jnp.concatenate([r[:, :width] for r in rows], axis=0)
    for i in range(4):
        gate = mm(x, gates[i][...])
        up = mm(x, ups[i][...])
        out_ref[:, i * part : (i + 1) * part] = (gate / (1.0 + jnp.exp(-gate)) * up).astype(bf16)


def contract_body(h_ref, d0, d1, d2, d3, *out_refs, first):
    cap = out_refs[0].shape[0]
    count = cap * len(out_refs)
    part = d0.shape[0]
    total = None
    for i, d in enumerate((d0, d1, d2, d3)):
        got = mm(h_ref[first : first + count, i * part : (i + 1) * part], d[...])
        total = got if total is None else total + got
    for k, ref in enumerate(out_refs):
        ref[...] = total[k * cap : (k + 1) * cap].astype(bf16)


def join_body(zy_ref, own_ref, other_ref, extra_ref, out_ref):
    extra = extra_ref[...].astype(f32)
    zero = extra[:, 0:1] + extra[:, 2:3]
    one = extra[:, 1:2] + extra[:, 3:4]
    odd = zy_ref[1] == 1
    mine = jnp.where(odd, one, zero)
    theirs = jnp.where(odd, zero, one)
    out_ref[...] = (own_ref[...].astype(f32) * mine + other_ref[...].astype(f32) * theirs).astype(bf16)


def restore_body(turn_ref, *refs):
    out_ref = refs[-1]
    cap = refs[0].shape[0]
    total = None
    for k, ref in enumerate(refs[:-1]):
        got = mm(turn_ref[:, k * cap : (k + 1) * cap], ref[...])
        total = got if total is None else total + got
    out_ref[...] = total.astype(bf16)


def paired_experts(moe_input, moe_gain, expert_pick, route_weight, gates, ups, downs):
    tokens, width = moe_input.shape
    ep_count = lax.axis_size("ep")
    ep_index = lax.axis_index("ep")
    cap = GROUPS * tokens // ep_count
    zy = jnp.stack([ep_index // TOPK, ep_index % TOPK]).astype(jnp.int32)

    def along(k):
        return [(i, i ^ (k * TOPK)) for i in range(ep_count)]

    across = [(i, i ^ 1) for i in range(ep_count)]
    row_type = jax.ShapeDtypeStruct((cap, width + LANES), bf16)
    wide_type = jax.ShapeDtypeStruct((cap, width), bf16)
    *sent, turn = call(
        functools.partial(route_body, cap=cap),
        "route",
        [row_type] * GROUPS + [jax.ShapeDtypeStruct((tokens, GROUPS * cap), bf16)],
        [SMEM] + [VMEM] * 5,
        32,
    )(zy, moe_input, moe_gain.reshape(1, width), expert_pick.T, expert_pick, route_weight)
    own = [sent[0]] + [lax.ppermute(sent[k], "ep", along(k)) for k in range(1, GROUPS)]
    theirs = [lax.ppermute(rows, "ep", across) for rows in own]
    part = gates[0].shape[2]
    count = 2 * GROUPS * cap
    hidden = call(
        expand_body,
        "expand",
        jax.ShapeDtypeStruct((count, 4 * part), bf16),
        [VMEM] * 16,
        48,
        flops=4 * count * width * 4 * part,
    )(*theirs, *own, *[g[0] for g in gates], *[u[0] for u in ups])
    results = [
        call(
            functools.partial(contract_body, first=i * GROUPS * cap),
            "contract",
            [wide_type] * GROUPS,
            [VMEM] * 5,
            48,
            flops=count * width * 4 * part,
        )(hidden, *[d[0] for d in downs])
        for i in range(2)
    ]
    others = [None] * GROUPS
    returned = [None] * GROUPS
    for k in (2, 3, 1, 0):
        others[k] = lax.ppermute(results[0][k], "ep", across)
    for k in (2, 3, 1, 0):
        joined = pl.pallas_call(
            join_body,
            name="join",
            out_shape=wide_type,
            grid=(1,),
            in_specs=[
                SMEM,
                pl.BlockSpec((cap, width), lambda i: (0, 0)),
                pl.BlockSpec((cap, width), lambda i: (0, 0)),
                pl.BlockSpec((cap, LANES), lambda i: (0, width // LANES)),
            ],
            out_specs=pl.BlockSpec((cap, width), lambda i: (0, 0)),
        )(zy, results[1][k], others[k], own[k])
        returned[k] = lax.ppermute(joined, "ep", along(k)) if k else joined
    return call(
        restore_body,
        "restore",
        jax.ShapeDtypeStruct((tokens, width), bf16),
        [VMEM] * (GROUPS + 1),
        32,
    )(turn, *returned)


def expand(arrived, gate_weights, up_weights):
    gate_in = jnp.einsum("necm,emf->necf", arrived, gate_weights, preferred_element_type=f32)
    up_in = jnp.einsum("necm,emf->necf", arrived, up_weights, preferred_element_type=f32)
    return (jax.nn.silu(gate_in) * up_in).astype(bf16)


def contract(hidden, down_weights):
    return jnp.einsum("necf,efm->necm", hidden, down_weights, preferred_element_type=f32)


def any_experts(moe_input, moe_gain, expert_pick, route_weight, w_gate, w_up, w_down):
    ep_count = lax.axis_size("ep")
    token_count = moe_input.shape[0]
    widened = moe_input.astype(f32)
    normed = (
        widened
        * lax.rsqrt(jnp.mean(widened * widened, axis=1, keepdims=True) + norm_eps)
        * moe_gain
    ).astype(bf16)
    local_experts = w_gate.shape[0]
    expert_total = local_experts * ep_count
    capacity = GROUPS * token_count // expert_total
    picks = expert_pick.reshape(-1)
    matches = (picks[:, None] == jnp.arange(expert_total, dtype=jnp.int32)[None, :]).astype(
        jnp.int32
    )
    ranks = jnp.sum((jnp.cumsum(matches, axis=0) - matches) * matches, axis=1)
    slots = picks * capacity + ranks
    owners = jnp.arange(picks.shape[0], dtype=jnp.int32) // TOPK
    table = jnp.full((expert_total * capacity,), token_count, jnp.int32).at[slots].set(owners)
    padded = jnp.concatenate([normed, jnp.zeros((1, normed.shape[1]), bf16)], axis=0)
    outgoing = padded[table].reshape(ep_count, local_experts, capacity, normed.shape[1])
    arrived = lax.all_to_all(outgoing, "ep", split_axis=0, concat_axis=0, tiled=True)
    gate_all, up_all, down_all = (
        lax.all_gather(w_gate, "tp", axis=2, tiled=True),
        lax.all_gather(w_up, "tp", axis=2, tiled=True),
        lax.all_gather(w_down, "tp", axis=1, tiled=True),
    )
    served = contract(expand(arrived, gate_all, up_all), down_all).astype(bf16)
    returned = lax.all_to_all(served, "ep", split_axis=0, concat_axis=0, tiled=True)
    flat = returned.reshape(expert_total * capacity, returned.shape[3])
    chosen = flat[slots].reshape(token_count, TOPK, flat.shape[1]).astype(f32)
    return jnp.sum(chosen * route_weight[:, :, None], axis=1).astype(bf16)


def local(
    query_rows,
    key_rows,
    value_rows,
    key_bias,
    out_weight,
    moe_input,
    moe_gain,
    expert_pick,
    route_weight,
    w_gate,
    w_up,
    w_down,
):
    tp_size = lax.axis_size("tp")
    ep_count = lax.axis_size("ep")
    paired = w_gate.shape[0] == 1 and ep_count == GROUPS * TOPK
    if paired:
        gates = spread(w_gate, tp_size)
        ups = spread(w_up, tp_size)
        downs = spread(w_down, tp_size)
    out_pieces = spread(out_weight, tp_size)
    mixer_out = mixer(query_rows, key_rows, value_rows, key_bias, out_pieces)
    if paired:
        routed_out = paired_experts(
            moe_input, moe_gain, expert_pick, route_weight, gates, ups, downs
        )
    else:
        routed_out = any_experts(
            moe_input, moe_gain, expert_pick, route_weight, w_gate, w_up, w_down
        )
    return (mixer_out, routed_out)


def solution(mesh):
    placed = (
        P("ep", "tp"),
        P("ep", "tp"),
        P("ep", "tp"),
        P(None, "tp"),
        P("tp", None),
        P(("ep", "tp"), None),
        P(),
        P(("ep", "tp"), None),
        P(("ep", "tp"), None),
        P("ep", None, "tp"),
        P("ep", None, "tp"),
        P("ep", "tp", None),
    )
    return jax.shard_map(
        local,
        mesh=mesh,
        in_specs=placed,
        out_specs=(P(("ep", "tp"), None), P(("ep", "tp"), None)),
        check_vma=False,
    )
```

time: 593 us -> 191 us (0.32)
  starting transfers between devices: 266 us -> 37.2 us
  waiting for transfers between devices: 201 us -> 65.7 us
  Pallas kernels: 0 us -> 56.8 us
  other arithmetic: 35 us -> 1.05 us
  loops' own time: 27.1 us -> 0 us
  matrix products: 23 us -> 0 us
  between operations: 14.5 us -> 0.86 us
  local copies, waits for them, and re-layouts: 20.9 us -> 27.9 us
    all_to_all x2, starting transfers between devices: 266 us -> 11.8 us  [the longest x1 6.98 us: mixer(): lax.all_to_all(outgoing, 'ep', split_axis=0, concat_axis=0, tiled=True)]
    all_gather x5 -> x0, waiting for transfers between devices: 151 us -> none  [the longest x1 67.5 us: local(): lax.all_gather(key_rows, 'ep', axis=0, tiled=True)]
    ppermute x0 -> x26, waiting for transfers between devices: none -> 65.7 us  [the longest x4 25.7 us: spread(): far = lax.ppermute(piece, 'tp', cross)]
    pallas_call x0 -> x12, Pallas kernels: none -> 56.8 us  [the longest x1 27.3 us: mixer(): call(functools.partial(attend_body, rows=rows, sub=sub, parts=parts), 'at...]
    all_to_all x2, waiting for transfers between devices: 48.2 us -> 0.01 us  [the longest x1 0.01 us: mixer(): lax.all_to_all(attended, ('ep', 'tp'), split_axis=0, concat_axis=0, tiled...]
    another operation x1 -> x0, loops' own time: 27.1 us -> none  [held_attend(): lax.fori_loop(0, top_block - seq_base + 1, visit, (zero_sum, zero_run))[0]]
    ppermute x0 -> x26, starting transfers between devices: none -> 25.4 us  [the longest x4 6.14 us: spread(): far = lax.ppermute(piece, 'tp', cross)]
    unnamed x15 -> x72, local copies, waits for them, and re-layouts: 4.76 us -> 27.9 us
  transfers between devices with their start and end apart: 8 -> 28, of which waited for: 4 -> 11; matrix products, arithmetic and copies ran while one was open for 13% -> 1% of each run, Pallas kernels for 0% -> 27%
where the time goes in v1:
time: 191 us; the launch traced here: 189 us
  waiting for transfers between devices  65.7 us (34%)
  Pallas kernels  56.8 us (30%)
  starting transfers between devices  37.2 us (19%)
  local copies, waits for them, and re-layouts  27.9 us (15%)
    unnamed x72, local copies, waits for them, and re-layouts  27.9 us
    pallas_call x1, Pallas kernels, mixer(): call(functools.partial(attend_body, rows=rows, sub=sub, parts=parts), 'at...  27.3 us
    ppermute x4, waiting for transfers between devices, spread(): far = lax.ppermute(piece, 'tp', cross)  25.7 us
    ppermute x3, waiting for transfers between devices, paired_experts(): returned[k] = lax.ppermute(joined, 'ep', along(k)) if k else joined  16 us
    ppermute x3, waiting for transfers between devices, paired_experts(): lax.ppermute(sent[k], 'ep', along(k))  14.9 us
    pallas_call x4, Pallas kernels, paired_experts(): pl.pallas_call(join_body, name='join', out_shape=wide_type, grid=(1,), in...  8.2 us
    pallas_call x1, Pallas kernels, paired_experts(): call(expand_body, 'expand', jax.ShapeDtypeStruct((count, 4 * part), bf16)...  7.62 us
    all_to_all x1, starting transfers between devices, mixer(): lax.all_to_all(outgoing, 'ep', split_axis=0, concat_axis=0, tiled=True)  6.98 us
  transfers between devices with their start and end apart: 28, of which 11 were waited for; matrix products, arithmetic and copies ran while one was open for 1% of the time, Pallas kernels for 27%

profile of v1, /device:TPU:0, one launch (start us, length us, event | category | flops | bytes accessed | tf_op | source)
XLA Modules:
  0.0 189.5 jit_solution(6277819969274201667)
XLA Ops:
  6.0 3.1 %collective-permute-start.4 = (bf16[64,2176]{1,0:T(8,128)(2,1)S(1)}, bf16[64,2176]{1,0:T(8,128)(2,1)S(1)}, u32[]{:S(2)}, u32[]{:S(2)}) collective-permute-start(bf16[64,2176]{1,0:T(8,128)(2,1)S(1)} %get-tuple-element.17), channel_id=1, source_target_pairs={{0,8},{4,12},{8,0},{12,4},{16,24},{20,28},{24,16},{28,20},{1,9},{5... | collective-permute-start | bytes 835592 | tf_op jit(solution)/shard_map/ppermute | solution.py:308
  9.1 2.6 %collective-permute-start.6 = (bf16[64,2176]{1,0:T(8,128)(2,1)S(1)}, bf16[64,2176]{1,0:T(8,128)(2,1)S(1)}, u32[]{:S(2)}, u32[]{:S(2)}) collective-permute-start(bf16[64,2176]{1,0:T(8,128)(2,1)S(1)} %get-tuple-element.18), channel_id=1, source_target_pairs={{0,16},{4,20},{8,24},{12,28},{16,0},{20,4},{24,8},{28,12},{1,17},{... | collective-permute-start | bytes 835592 | tf_op jit(solution)/shard_map/ppermute | solution.py:308
  11.7 1.7 collective-permute-start.3
  14.9 6.1 %collective-permute-done.4.refs_5_.extra_ref = bf16[64,2176]{1,0:T(8,128)(2,1)S(1)} collective-permute-done((bf16[64,2176]{1,0:T(8,128)(2,1)S(1)}, bf16[64,2176]{1,0:T(8,128)(2,1)S(1)}, u32[]{:S(2)}, u32[]{:S(2)}) %collective-permute-start.4) | collective-permute-done | bytes 278560 | tf_op jit(solution)/shard_map/ppermute | solution.py:308
  22.6 8.8 %collective-permute-done.6.refs_6_.extra_ref = bf16[64,2176]{1,0:T(8,128)(2,1)S(1)} collective-permute-done((bf16[64,2176]{1,0:T(8,128)(2,1)S(1)}, bf16[64,2176]{1,0:T(8,128)(2,1)S(1)}, u32[]{:S(2)}, u32[]{:S(2)}) %collective-permute-start.6) | collective-permute-done | bytes 278560 | tf_op jit(solution)/shard_map/ppermute | solution.py:308
  37.8 2.6 %collective-permute-done.5.refs_1_ = bf16[64,2176]{1,0:T(8,128)(2,1)S(1)} collective-permute-done((bf16[64,2176]{1,0:T(8,128)(2,1)S(1)}, bf16[64,2176]{1,0:T(8,128)(2,1)S(1)}, u32[]{:S(2)}, u32[]{:S(2)}) %collective-permute-start.5) | collective-permute-done | bytes 278560 | tf_op jit(solution)/shard_map/ppermute | solution.py:309
  41.1 2.3 %collective-permute-done.7.refs_2_ = bf16[64,2176]{1,0:T(8,128)(2,1)S(1)} collective-permute-done((bf16[64,2176]{1,0:T(8,128)(2,1)S(1)}, bf16[64,2176]{1,0:T(8,128)(2,1)S(1)}, u32[]{:S(2)}, u32[]{:S(2)}) %collective-permute-start.7) | collective-permute-done | bytes 278560 | tf_op jit(solution)/shard_map/ppermute | solution.py:309
  51.3 7.0 %all-to-all-start = ((bf16[8,640,128]{2,1,0:T(8,128)(2,1)}), bf16[8,640,128]{2,1,0:T(8,128)(2,1)}, u32[]{:S(2)}, u32[]{:S(2)}) async-start(bf16[8,640,128]{2,1,0:T(8,128)(2,1)} %pack.1), calls=%async_computation | async-start | bytes 2621440 | tf_op jit(solution)/shard_map/all_to_all | solution.py:179
  58.6 3.6 %collective-permute-done.11 = bf16[1,2048,256]{2,1,0:T(8,128)(2,1)} collective-permute-done((bf16[1,2048,256]{2,1,0:T(8,128)(2,1)}, bf16[1,2048,256]{2,1,0:T(8,128)(2,1)}, u32[]{:S(2)}, u32[]{:S(2)}) %collective-permute-start.11) | collective-permute-done | bytes 1048608 | tf_op jit(solution)/shard_map/ppermute | solution.py:156
  62.7 19.7 %collective-permute-done.17 = bf16[1,256,2048]{2,1,0:T(8,128)(2,1)S(1)} collective-permute-done((bf16[1,256,2048]{2,1,0:T(8,128)(2,1)}, bf16[1,256,2048]{2,1,0:T(8,128)(2,1)S(1)}, u32[]{:S(2)}, u32[]{:S(2)}) %collective-permute-start.17) | collective-permute-done | bytes 1048608 | tf_op jit(solution)/shard_map/ppermute | solution.py:156
  93.2 7.6 %expand.1.h_ref = bf16[512,1024]{1,0:T(8,128)(2,1)S(1)} custom-call(bf16[64,2176]{1,0:T(8,128)(2,1)S(1)} %copy-done.25, bf16[64,2176]{1,0:T(8,128)(2,1)S(1)} %copy-done.27, bf16[64,2176]{1,0:T(8,128)(2,1)S(1)} %copy-done.29, bf16[64,2176]{1,0:T(8,128)(2,1)S(1)} %copy-done.31, bf16[64,2176]{1,0:T(8,128)(2,1)S(1)} %get-tuple-element.16.refs_4_.extra_ref, ...), custom_call_target="tpu_custom_call" | custom-call | flops 4294967296 | tf_op jit(solution)/shard_map/expand/pallas_call | solution.py:312
  102.0 3.4 %contract.3 = (bf16[64,2048]{1,0:T(8,128)(2,1)}, bf16[64,2048]{1,0:T(8,128)(2,1)}, bf16[64,2048]{1,0:T(8,128)(2,1)}, bf16[64,2048]{1,0:T(8,128)(2,1)S(1)}) custom-call(bf16[512,1024]{1,0:T(8,128)(2,1)S(1)} %expand.1.h_ref, bf16[256,2048]{1,0:T(8,128)(2,1)S(1)} %bitcast.18, bf16[256,2048]{1,0:T(8,128)(2,1)S(1)} %bitcast.22, bf16[256,2048]{1,0:T(8,128)(2,1)S(1)} %bitcast.20, ...), custom_call_target="tpu_custom_call" | custom-call | flops 1073741824 | tf_op jit(solution)/shard_map/contract/pallas_call | solution.py:321
  105.8 2.4 %collective-permute-done.1.w2 = bf16[256,2048]{1,0:T(8,128)(2,1)} collective-permute-done((bf16[256,2048]{1,0:T(8,128)(2,1)}, bf16[256,2048]{1,0:T(8,128)(2,1)}, u32[]{:S(2)}, u32[]{:S(2)}) %collective-permute-start.1) | collective-permute-done | bytes 1048608 | tf_op jit(solution)/shard_map/ppermute | solution.py:156
  111.3 3.3 %collective-permute-done.24.other_ref = bf16[64,2048]{1,0:T(8,128)(2,1)} collective-permute-done((bf16[64,2048]{1,0:T(8,128)(2,1)S(1)}, bf16[64,2048]{1,0:T(8,128)(2,1)}, u32[]{:S(2)}, u32[]{:S(2)}) %collective-permute-start.24) | collective-permute-done | bytes 262176 | tf_op jit(solution)/shard_map/ppermute | solution.py:334
  115.1 27.3 %attend.1 = bf16[8,4,32,128]{3,2,1,0:T(8,128)(2,1)S(1)} custom-call(s32[2]{0:T(128)S(1)} %pad_add_fusion.where_ref, bf16[8,640,128]{2,1,0:T(8,128)(2,1)} %all-to-all-done.got_ref, f32[16,256]{1,0:T(8,128)S(1)} %mul.12.bias_ref), custom_call_target="tpu_custom_call" | custom-call | flops 3221225472 | tf_op jit(solution)/shard_map/attend/pallas_call | solution.py:184
  143.2 4.9 %all-to-all-start.1 = ((bf16[32,32,128]{2,1,0:T(8,128)(2,1)}), bf16[32,32,128]{2,1,0:T(8,128)(2,1)S(1)}, u32[]{:S(2)}, u32[]{:S(2)}) async-start(bf16[32,32,128]{2,1,0:T(8,128)(2,1)} %bitcast.24), calls=%async_computation.1 | async-start | bytes 524288 | tf_op jit(solution)/shard_map/all_to_all | solution.py:193
  149.3 2.5 %contract.2 = (bf16[64,2048]{1,0:T(8,128)(2,1)S(1)}, bf16[64,2048]{1,0:T(8,128)(2,1)S(1)}, bf16[64,2048]{1,0:T(8,128)(2,1)S(1)}, bf16[64,2048]{1,0:T(8,128)(2,1)S(1)}) custom-call(bf16[512,1024]{1,0:T(8,128)(2,1)S(1)} %copy-done.2, bf16[256,2048]{1,0:T(8,128)(2,1)S(1)} %bitcast.19, bf16[256,2048]{1,0:T(8,128)(2,1)S(1)} %bitcast.23, ...), custom_call_target="tpu_custom_call" | custom-call | flops 1073741824 | tf_op jit(solution)/shard_map/contract/pallas_call | solution.py:321
  154.6 2.0 %join.7 = bf16[64,2048]{1,0:T(8,128)(2,1)} custom-call(s32[2]{0:T(128)} %copy-done.20, bf16[64,2048]{1,0:T(8,128)(2,1)} %copy-done.16, bf16[64,2048]{1,0:T(8,128)(2,1)} %collective-permute-done.24.other_ref, bf16[64,2176]{1,0:T(8,128)(2,1)} %copy-done.10), custom_call_target="tpu_custom_call" | custom-call | tf_op jit(solution)/shard_map/join/pallas_call | solution.py:336
  156.6 3.6 %collective-permute-start.25 = (bf16[64,2048]{1,0:T(8,128)(2,1)}, bf16[64,2048]{1,0:T(8,128)(2,1)S(1)}, u32[]{:S(2)}, u32[]{:S(2)}) collective-permute-start(bf16[64,2048]{1,0:T(8,128)(2,1)} %join.7), channel_id=1, source_target_pairs={{0,24},{4,28},{8,16},{12,20},{16,8},{20,12},{24,0},{28,4},{1,25},{... | collective-permute-start | bytes 786440 | tf_op jit(solution)/shard_map/ppermute | solution.py:349
  160.3 2.0 %join.6 = bf16[64,2048]{1,0:T(8,128)(2,1)} custom-call(s32[2]{0:T(128)} %copy-done.20, bf16[64,2048]{1,0:T(8,128)(2,1)} %copy-done.15, bf16[64,2048]{1,0:T(8,128)(2,1)} %collective-permute-done.22.other_ref, bf16[64,2176]{1,0:T(8,128)(2,1)} %copy-done.8), custom_call_target="tpu_custom_call" | custom-call | tf_op jit(solution)/shard_map/join/pallas_call | solution.py:336
  162.3 2.1 %join.5 = bf16[64,2048]{1,0:T(8,128)(2,1)} custom-call(s32[2]{0:T(128)} %copy-done.20, bf16[64,2048]{1,0:T(8,128)(2,1)} %copy-done.14, bf16[64,2048]{1,0:T(8,128)(2,1)} %collective-permute-done.20.other_ref, bf16[64,2176]{1,0:T(8,128)(2,1)} %copy-done.6), custom_call_target="tpu_custom_call" | custom-call | tf_op jit(solution)/shard_map/join/pallas_call | solution.py:336
  165.1 2.1 %join.4.refs_0_ = bf16[64,2048]{1,0:T(8,128)(2,1)} custom-call(s32[2]{0:T(128)} %copy-done.20, bf16[64,2048]{1,0:T(8,128)(2,1)} %copy-done.13, bf16[64,2048]{1,0:T(8,128)(2,1)} %collective-permute-done.19.other_ref, bf16[64,2176]{1,0:T(8,128)(2,1)} %copy-done.5), custom_call_target="tpu_custom_call" | custom-call | tf_op jit(solution)/shard_map/join/pallas_call | solution.py:336
  167.9 15.3 %collective-permute-done.23.refs_2_ = bf16[64,2048]{1,0:T(8,128)(2,1)S(1)} collective-permute-done((bf16[64,2048]{1,0:T(8,128)(2,1)}, bf16[64,2048]{1,0:T(8,128)(2,1)S(1)}, u32[]{:S(2)}, u32[]{:S(2)}) %collective-permute-start.23) | collective-permute-done | bytes 262176 | tf_op jit(solution)/shard_map/ppermute | solution.py:349
  185.7 3.8 %project.1 = bf16[128,2048]{1,0:T(8,128)(2,1)} custom-call(s32[2]{0:T(128)S(1)} %pad_add_fusion.where_ref, bf16[32,32,128]{2,1,0:T(8,128)(2,1)S(1)} %all-to-all-done.1.got_ref, bf16[256,2048]{1,0:T(8,128)(2,1)} %w0.1, bf16[256,2048]{1,0:T(8,128)(2,1)} %collective-permute-done.w1, bf16[256,2048]{1,0:T(8,128)(2,1)} %collective-permute-done.1.w2, ...), custom_call_target="tpu_custom_call" | custom-call | flops 536870912 | tf_op jit(solution)/shard_map/project/pallas_call | solution.py:194
  (120 shorter events, 48.9 us)
Async XLA Ops:
  6.0 15.0 %collective-permute-start.4 = (bf16[64,2176]{1,0:T(8,128)(2,1)S(1)}, bf16[64,2176]{1,0:T(8,128)(2,1)S(1)}, u32[]{:S(2)}, u32[]{:S(2)}) collective-permute-start(bf16[64,2176]{1,0:T(8,128)(2,1)S(1)} %get-tuple-element.17), channel_id=1, source_target_pairs={{0,8},{4,12},{8,0},{12,4},{16,24},{20,28},{24,16},{28,20},{1,9},{5... | collective-permute-start | bytes 835592 | tf_op jit(solution)/shard_map/ppermute | solution.py:308
  9.1 22.4 %collective-permute-start.6 = (bf16[64,2176]{1,0:T(8,128)(2,1)S(1)}, bf16[64,2176]{1,0:T(8,128)(2,1)S(1)}, u32[]{:S(2)}, u32[]{:S(2)}) collective-permute-start(bf16[64,2176]{1,0:T(8,128)(2,1)S(1)} %get-tuple-element.18), channel_id=1, source_target_pairs={{0,16},{4,20},{8,24},{12,28},{16,0},{20,4},{24,8},{28,12},{1,17},{... | collective-permute-start | bytes 835592 | tf_op jit(solution)/shard_map/ppermute | solution.py:308
  11.7 22.0 %collective-permute-start.8 = (bf16[64,2176]{1,0:T(8,128)(2,1)S(1)}, bf16[64,2176]{1,0:T(8,128)(2,1)S(1)}, u32[]{:S(2)}, u32[]{:S(2)}) collective-permute-start(bf16[64,2176]{1,0:T(8,128)(2,1)S(1)} %get-tuple-element.19), channel_id=1, source_target_pairs={{0,24},{4,28},{8,16},{12,20},{16,8},{20,12},{24,0},{28,4},{1,25},{... | collective-permute-start | bytes 835592 | tf_op jit(solution)/shard_map/ppermute | solution.py:308
  11.7 23.2 %collective-permute-start.3 = (bf16[64,2176]{1,0:T(8,128)(2,1)S(1)}, bf16[64,2176]{1,0:T(8,128)(2,1)S(1)}, u32[]{:S(2)}, u32[]{:S(2)}) collective-permute-start(bf16[64,2176]{1,0:T(8,128)(2,1)S(1)} %get-tuple-element.16.refs_4_.extra_ref), channel_id=1, source_target_pairs={{0,4},{4,0},{8,12},{12,8},{16,20},{20,16},{24,28},{28,24},{1,5},{5... | collective-permute-start | bytes 835592 | tf_op jit(solution)/shard_map/ppermute | solution.py:309
  13.4 44.9 %collective-permute-start.14 = (bf16[1,2048,256]{2,1,0:T(8,128)(2,1)}, bf16[1,2048,256]{2,1,0:T(8,128)(2,1)}, u32[]{:S(2)}, u32[]{:S(2)}) collective-permute-start(bf16[1,2048,256]{2,1,0:T(8,128)(2,1)} %param.22), channel_id=1, source_target_pairs={{0,2},{1,3},{2,0},{3,1},{4,6},{5,7},{6,4},{7,5},{8,10},{9,11},{10,... | collective-permute-start | bytes 3145736 | tf_op jit(solution)/shard_map/ppermute | solution.py:156
  21.0 41.3 %collective-permute-start.11 = (bf16[1,2048,256]{2,1,0:T(8,128)(2,1)}, bf16[1,2048,256]{2,1,0:T(8,128)(2,1)}, u32[]{:S(2)}, u32[]{:S(2)}) collective-permute-start(bf16[1,2048,256]{2,1,0:T(8,128)(2,1)} %param.21), channel_id=1, source_target_pairs={{0,2},{1,3},{2,0},{3,1},{4,6},{5,7},{6,4},{7,5},{8,10},{9,11},{10,... | collective-permute-start | bytes 3145736 | tf_op jit(solution)/shard_map/ppermute | solution.py:156
  41.1 21.1 %collective-permute-start.13 = (bf16[1,2048,256]{2,1,0:T(8,128)(2,1)}, bf16[1,2048,256]{2,1,0:T(8,128)(2,1)}, u32[]{:S(2)}, u32[]{:S(2)}) collective-permute-start(bf16[1,2048,256]{2,1,0:T(8,128)(2,1)} %param.22), channel_id=1, source_target_pairs={{0,1},{1,0},{2,3},{3,2},{4,5},{5,4},{6,7},{7,6},{8,9},{9,8},{10,11... | collective-permute-start | bytes 3145736 | tf_op jit(solution)/shard_map/ppermute | solution.py:157
  44.1 38.3 %collective-permute-start.17 = (bf16[1,256,2048]{2,1,0:T(8,128)(2,1)}, bf16[1,256,2048]{2,1,0:T(8,128)(2,1)S(1)}, u32[]{:S(2)}, u32[]{:S(2)}) collective-permute-start(bf16[1,256,2048]{2,1,0:T(8,128)(2,1)} %param.23), channel_id=1, source_target_pairs={{0,2},{1,3},{2,0},{3,1},{4,6},{5,7},{6,4},{7,5},{8,10},{9,11},{10,... | collective-permute-start | bytes 3145736 | tf_op jit(solution)/shard_map/ppermute | solution.py:156
  47.1 35.3 %collective-permute-start.10 = (bf16[1,2048,256]{2,1,0:T(8,128)(2,1)}, bf16[1,2048,256]{2,1,0:T(8,128)(2,1)}, u32[]{:S(2)}, u32[]{:S(2)}) collective-permute-start(bf16[1,2048,256]{2,1,0:T(8,128)(2,1)} %param.21), channel_id=1, source_target_pairs={{0,1},{1,0},{2,3},{3,2},{4,5},{5,4},{6,7},{7,6},{8,9},{9,8},{10,11... | collective-permute-start | bytes 3145736 | tf_op jit(solution)/shard_map/ppermute | solution.py:157
  51.3 63.8 %all-to-all-start = ((bf16[8,640,128]{2,1,0:T(8,128)(2,1)}), bf16[8,640,128]{2,1,0:T(8,128)(2,1)}, u32[]{:S(2)}, u32[]{:S(2)}) async-start(bf16[8,640,128]{2,1,0:T(8,128)(2,1)} %pack.1), calls=%async_computation | async-start | bytes 2621440 | tf_op jit(solution)/shard_map/all_to_all | solution.py:179
  58.3 25.6 %collective-permute-start.15 = (bf16[1,2048,256]{2,1,0:T(8,128)(2,1)}, bf16[1,2048,256]{2,1,0:T(8,128)(2,1)S(1)}, u32[]{:S(2)}, u32[]{:S(2)}) collective-permute-start(bf16[1,2048,256]{2,1,0:T(8,128)(2,1)} %collective-permute-done.14), channel_id=1, source_target_pairs={{0,1},{1,0},{2,3},{3,2},{4,5},{5,4},{6,7},{7,6},{8,9},{9,8},{10,11... | collective-permute-start | bytes 3145736 | tf_op jit(solution)/shard_map/ppermute | solution.py:158
  62.2 21.7 %collective-permute-start.12 = (bf16[1,2048,256]{2,1,0:T(8,128)(2,1)}, bf16[1,2048,256]{2,1,0:T(8,128)(2,1)S(1)}, u32[]{:S(2)}, u32[]{:S(2)}) collective-permute-start(bf16[1,2048,256]{2,1,0:T(8,128)(2,1)} %collective-permute-done.11), channel_id=1, source_target_pairs={{0,1},{1,0},{2,3},{3,2},{4,5},{5,4},{6,7},{7,6},{8,9},{9,8},{10,11... | collective-permute-start | bytes 3145736 | tf_op jit(solution)/shard_map/ppermute | solution.py:158
  62.2 38.6 %collective-permute-start.16 = (bf16[1,256,2048]{2,1,0:T(8,128)(2,1)S(1)}, bf16[1,256,2048]{2,1,0:T(8,128)(2,1)S(1)}, u32[]{:S(2)}, u32[]{:S(2)}) collective-permute-start(bf16[1,256,2048]{2,1,0:T(8,128)(2,1)S(1)} %copy-done), channel_id=1, source_target_pairs={{0,1},{1,0},{2,3},{3,2},{4,5},{5,4},{6,7},{7,6},{8,9},{9,8},{10,11... | collective-permute-start | bytes 3145736 | tf_op jit(solution)/shard_map/ppermute | solution.py:157
  82.4 18.4 %collective-permute-start.18 = (bf16[1,256,2048]{2,1,0:T(8,128)(2,1)S(1)}, bf16[1,256,2048]{2,1,0:T(8,128)(2,1)S(1)}, u32[]{:S(2)}, u32[]{:S(2)}) collective-permute-start(bf16[1,256,2048]{2,1,0:T(8,128)(2,1)S(1)} %collective-permute-done.17), channel_id=1, source_target_pairs={{0,1},{1,0},{2,3},{3,2},{4,5},{5,4},{6,7},{7,6},{8,9},{9,8},{10,11... | collective-permute-start | bytes 3145736 | tf_op jit(solution)/shard_map/ppermute | solution.py:158
  82.4 25.9 %collective-permute-start.1 = (bf16[256,2048]{1,0:T(8,128)(2,1)}, bf16[256,2048]{1,0:T(8,128)(2,1)}, u32[]{:S(2)}, u32[]{:S(2)}) collective-permute-start(bf16[256,2048]{1,0:T(8,128)(2,1)} %w0.1), channel_id=1, source_target_pairs={{0,2},{1,3},{2,0},{3,1},{4,6},{5,7},{6,4},{7,5},{8,10},{9,11},{10,... | collective-permute-start | bytes 3145736 | tf_op jit(solution)/shard_map/ppermute | solution.py:156
  105.8 79.9 %collective-permute-start = (bf16[256,2048]{1,0:T(8,128)(2,1)}, bf16[256,2048]{1,0:T(8,128)(2,1)}, u32[]{:S(2)}, u32[]{:S(2)}) collective-permute-start(bf16[256,2048]{1,0:T(8,128)(2,1)} %w0.1), channel_id=1, source_target_pairs={{0,1},{1,0},{2,3},{3,2},{4,5},{5,4},{6,7},{7,6},{8,9},{9,8},{10,11... | collective-permute-start | bytes 3145736 | tf_op jit(solution)/shard_map/ppermute | solution.py:157
  108.3 77.4 %collective-permute-start.2 = (bf16[256,2048]{1,0:T(8,128)(2,1)}, bf16[256,2048]{1,0:T(8,128)(2,1)}, u32[]{:S(2)}, u32[]{:S(2)}) collective-permute-start(bf16[256,2048]{1,0:T(8,128)(2,1)} %collective-permute-done.1.w2), channel_id=1, source_target_pairs={{0,1},{1,0},{2,3},{3,2},{4,5},{5,4},{6,7},{7,6},{8,9},{9,8},{10,11... | collective-permute-start | bytes 3145736 | tf_op jit(solution)/shard_map/ppermute | solution.py:158
  109.3 47.4 %collective-permute-start.22 = (bf16[64,2048]{1,0:T(8,128)(2,1)}, bf16[64,2048]{1,0:T(8,128)(2,1)}, u32[]{:S(2)}, u32[]{:S(2)}) collective-permute-start(bf16[64,2048]{1,0:T(8,128)(2,1)} %get-tuple-element.25), channel_id=1, source_target_pairs={{0,4},{4,0},{8,12},{12,8},{16,20},{20,16},{24,28},{28,24},{1,5},{5... | collective-permute-start | bytes 786440 | tf_op jit(solution)/shard_map/ppermute | solution.py:334
  109.8 52.5 %collective-permute-start.20 = (bf16[64,2048]{1,0:T(8,128)(2,1)}, bf16[64,2048]{1,0:T(8,128)(2,1)}, u32[]{:S(2)}, u32[]{:S(2)}) collective-permute-start(bf16[64,2048]{1,0:T(8,128)(2,1)} %get-tuple-element.23), channel_id=1, source_target_pairs={{0,4},{4,0},{8,12},{12,8},{16,20},{20,16},{24,28},{28,24},{1,5},{5... | collective-permute-start | bytes 786440 | tf_op jit(solution)/shard_map/ppermute | solution.py:334
  114.6 49.8 %collective-permute-start.19 = (bf16[64,2048]{1,0:T(8,128)(2,1)}, bf16[64,2048]{1,0:T(8,128)(2,1)}, u32[]{:S(2)}, u32[]{:S(2)}) collective-permute-start(bf16[64,2048]{1,0:T(8,128)(2,1)} %get-tuple-element.21), channel_id=1, source_target_pairs={{0,4},{4,0},{8,12},{12,8},{16,20},{20,16},{24,28},{28,24},{1,5},{5... | collective-permute-start | bytes 786440 | tf_op jit(solution)/shard_map/ppermute | solution.py:334
  143.2 42.5 %all-to-all-start.1 = ((bf16[32,32,128]{2,1,0:T(8,128)(2,1)}), bf16[32,32,128]{2,1,0:T(8,128)(2,1)S(1)}, u32[]{:S(2)}, u32[]{:S(2)}) async-start(bf16[32,32,128]{2,1,0:T(8,128)(2,1)} %bitcast.24), calls=%async_computation.1 | async-start | bytes 524288 | tf_op jit(solution)/shard_map/all_to_all | solution.py:193
  156.6 11.3 %collective-permute-start.25 = (bf16[64,2048]{1,0:T(8,128)(2,1)}, bf16[64,2048]{1,0:T(8,128)(2,1)S(1)}, u32[]{:S(2)}, u32[]{:S(2)}) collective-permute-start(bf16[64,2048]{1,0:T(8,128)(2,1)} %join.7), channel_id=1, source_target_pairs={{0,24},{4,28},{8,16},{12,20},{16,8},{20,12},{24,0},{28,4},{1,25},{... | collective-permute-start | bytes 786440 | tf_op jit(solution)/shard_map/ppermute | solution.py:349
  162.3 20.9 %collective-permute-start.23 = (bf16[64,2048]{1,0:T(8,128)(2,1)}, bf16[64,2048]{1,0:T(8,128)(2,1)S(1)}, u32[]{:S(2)}, u32[]{:S(2)}) collective-permute-start(bf16[64,2048]{1,0:T(8,128)(2,1)} %join.6), channel_id=1, source_target_pairs={{0,16},{4,20},{8,24},{12,28},{16,0},{20,4},{24,8},{28,12},{1,17},{... | collective-permute-start | bytes 786440 | tf_op jit(solution)/shard_map/ppermute | solution.py:349
  164.4 18.9 %collective-permute-start.21 = (bf16[64,2048]{1,0:T(8,128)(2,1)}, bf16[64,2048]{1,0:T(8,128)(2,1)S(1)}, u32[]{:S(2)}, u32[]{:S(2)}) collective-permute-start(bf16[64,2048]{1,0:T(8,128)(2,1)} %join.5), channel_id=1, source_target_pairs={{0,8},{4,12},{8,0},{12,4},{16,24},{20,28},{24,16},{28,20},{1,9},{5... | collective-permute-start | bytes 786440 | tf_op jit(solution)/shard_map/ppermute | solution.py:349
  (39 other events, 208.6 us)

commit v2 on v1

v2 whole, which is shorter than its diff:
```python
import functools
import math

import jax
import jax.numpy as jnp
from jax import lax
from jax.experimental import pallas as pl
from jax.experimental.pallas import tpu as pltpu
from jax.sharding import PartitionSpec as P


HEAD_DIM = 64
GROUPS = 4
TOPK = 2
LANES = 128
KEY_TILE = 256
LOG2E = math.log2(math.e)
MIB = 1 << 20

norm_eps = 1e-06
bf16 = jnp.bfloat16
f32 = jnp.float32

RETURN_ORDER = (2, 3, 1, 0)

VMEM = pl.BlockSpec(memory_space=pltpu.VMEM)


def whole(array):
    return pl.BlockSpec(array.shape, lambda i: (0,) * array.ndim)


def call(body, outs, ins, limit, flops=0, moved=0, scratch=()):
    return pl.pallas_call(
        body,
        out_shape=outs,
        scratch_shapes=scratch,
        grid=(1,),
        in_specs=ins,
        out_specs=jax.tree.map(lambda _: VMEM, outs),
        compiler_params=pltpu.CompilerParams(vmem_limit_bytes=limit * MIB),
        cost_estimate=pl.CostEstimate(flops=flops, bytes_accessed=moved, transcendentals=0),
    )


def exchange(piece, axes):
    return lax.all_to_all(piece, axes, split_axis=0, concat_axis=0, tiled=True)


def spot_of(sharers):
    ep = lax.axis_index("ep")
    return lax.rem(ep, sharers), lax.axis_index("tp"), lax.div(ep, sharers)


def mm(a, b):
    return jnp.dot(a, b, preferred_element_type=f32)


def pack_body(bias_any, q_ref, k_ref, v_ref, bias_ref, out_ref, *, heads, sharers, parts):
    bias_into(bias_any, bias_ref, spot_of(sharers)[2])
    rows = q_ref.shape[0]
    part_rows = rows // parts
    sub = part_rows // sharers
    half = rows // sharers // 2
    for h in range(heads):
        cols = pl.ds(h * HEAD_DIM, HEAD_DIM)
        pair = jnp.concatenate([k_ref[:, cols], v_ref[:, cols]], axis=1)
        for s in range(sharers):
            out_ref[h * sharers + s, :rows] = pair
            mine = jnp.concatenate(
                [q_ref[pl.ds(t * part_rows + s * sub, sub), cols] for t in range(parts)], axis=0
            )
            out_ref[h * sharers + s, rows:] = jnp.concatenate([mine[:half], mine[half:]], axis=1)


def bias_into(bias_any, out_ref, head):
    tiles, width = out_ref.shape
    line = bias_any[pl.ds(head, 1)] * LOG2E
    for i in range(tiles):
        out_ref[i : i + 1] = line[:, i * width : (i + 1) * width]


def pack_pair_body(bias_any, q_ref, k_ref, v_ref, bias_ref, *refs, heads, parts):
    out_refs, all_ref = refs[:-1], refs[-1]
    share, _, head = spot_of(TOPK)
    bias_into(bias_any, bias_ref, head)
    rows = q_ref.shape[0]
    part_rows = rows // parts
    sub = part_rows // TOPK
    half = rows // TOPK // 2
    second = share == 1
    for h in range(heads):
        cols = pl.ds(h * HEAD_DIM, HEAD_DIM)
        packed = []
        for s in range(TOPK):
            mine = jnp.concatenate(
                [q_ref[pl.ds(t * part_rows + s * sub, sub), cols] for t in range(parts)], axis=0
            )
            packed.append(jnp.concatenate([mine[:half], mine[half:]], axis=1))
        all_ref[h, :half] = jnp.where(second, packed[1], packed[0])
        all_ref[h, half : half + rows] = jnp.concatenate([k_ref[:, cols], v_ref[:, cols]], axis=1)
        all_ref[h, half + rows :] = jnp.where(second, packed[0], packed[1])
    for k, ref in enumerate(out_refs):
        ref[...] = all_ref[head ^ k]


def attend_pair_body(bias_ref, *refs, rows, sub, parts):
    arrived, out_refs = refs[: 2 * GROUPS], refs[2 * GROUPS : 3 * GROUPS]
    got_ref, *scratch = refs[3 * GROUPS :]
    half = sub * parts // 2
    y, _, z = spot_of(TOPK)
    for k in range(GROUPS):
        for side in range(2):
            ref = arrived[side * GROUPS + k]
            block = (z ^ k) * TOPK + (y ^ side)
            got_ref[block, :rows] = ref[half : half + rows]
            got_ref[block, rows:] = ref[half + rows :] if side else ref[:half]
    attend_body(got_ref, bias_ref, *out_refs, *scratch, rows=rows, sub=sub, parts=parts)


def attend_body(got_ref, bias_ref, *refs, rows, sub, parts):
    (*out_refs, acc_ref, run_ref, gap_ref, rest_ref, soft_ref, weight_ref, sum_ref, all_ref) = refs
    blocks = got_ref.shape[0]
    mine = sub * parts
    half = mine // 2
    share = spot_of(rows // mine)[0]
    scale = HEAD_DIM**-0.5 * LOG2E
    tiles = rows // KEY_TILE
    part_rows = rows // parts
    low = lax.broadcasted_iota(jnp.int32, (half, LANES), 1) < HEAD_DIM
    later = (
        lax.broadcasted_iota(jnp.int32, (KEY_TILE, KEY_TILE), 0)
        > lax.broadcasted_iota(jnp.int32, (KEY_TILE, KEY_TILE), 1)
    )
    after = jnp.where(later, 1.0, 0.0).astype(bf16)
    every = jnp.ones((KEY_TILE, KEY_TILE), bf16)

    def cut(c):
        return slice(c * KEY_TILE, (c + 1) * KEY_TILE)

    def query_of(b):
        packed = got_ref[b, pl.ds(rows, half)].astype(f32)
        return jnp.concatenate(
            [
                jnp.where(low, packed, 0.0),
                jnp.where(low, pltpu.roll(packed, HEAD_DIM, 1), 0.0),
            ],
            axis=0,
        ).astype(bf16)

    def causal(c):
        row = lax.broadcasted_iota(jnp.int32, (mine, KEY_TILE), 0)
        spot = row + share * sub
        for t in range(1, parts):
            spot = spot + jnp.where(row >= t * sub, part_rows - sub, 0)
        return lax.broadcasted_iota(jnp.int32, (mine, KEY_TILE), 1) + c * KEY_TILE < spot

    def soften(b, source, p, masked):
        query = query_of(b)
        for c in reversed(range(tiles)):
            raw = lax.dot_general(
                query,
                got_ref[source, cut(c)],
                (((1,), (1,)), ((), ())),
                preferred_element_type=f32,
            )
            score = raw * scale + bias_ref[pl.ds(source * tiles + c, 1)]
            soft = lax.log2(1.0 + jnp.exp2(jnp.minimum(score, 126.0)))
            soft = jnp.maximum(score, soft)
            gap = score - soft
            if masked:
                keep = causal(c)
                soft = jnp.where(keep, soft, 0.0)
                gap = jnp.where(keep, gap, -1e30)
            gap_ref[p, :, cut(c)] = gap
            soft_ref[p, :, cut(c)] = soft.astype(bf16)

    def total_up(p):
        for c in reversed(range(tiles)):
            rest = mm(soft_ref[p, :, cut(c)], after)
            for later_c in range(c + 1, tiles):
                rest = rest + mm(soft_ref[p, :, cut(later_c)], every)
            rest_ref[p, :, cut(c)] = rest
            if c == 0:
                sum_ref[p] = rest[:, :LANES] + soft_ref[p, :, :LANES].astype(f32)

    def weigh(p):
        for c in range(tiles):
            weight = jnp.exp2(gap_ref[p, :, cut(c)] - rest_ref[p, :, cut(c)])
            weight_ref[p, :, cut(c)] = weight.astype(bf16)
        all_ref[p] = jnp.broadcast_to(sum_ref[p, :, :1], (mine, LANES))

    def gather(b, source, p, valid, fresh):
        portion = mm(weight_ref[p], got_ref[source, :rows])
        total = all_ref[p]
        if fresh:
            acc = portion
            run = total
        else:
            run = run_ref[b]
            acc = acc_ref[b] + portion * jnp.exp2(-run)
            run = run + total
        acc_ref[b] = jnp.where(valid, acc, acc_ref[b])
        run_ref[b] = jnp.where(valid, run, run_ref[b])

    def diagonal(k, _):
        for p in range(2):
            i = 2 * k + p
            old = jnp.minimum(jnp.maximum(i - 3, 0), blocks - 1)
            now = jnp.minimum(i, blocks - 1)
            gather(old, old, 1 - p, (i >= 3) & (i < blocks + 3), True)
            weigh(p)
            total_up(1 - p)
            soften(now, now, p, True)
        return 0

    lax.fori_loop(0, (blocks + 4) // 2, diagonal, 0)
    count = blocks * (blocks - 1) // 2

    def step(k, state):
        for p in range(2):
            i = 2 * k + p
            gather(*state[0:2], 1 - p, (i >= 3) & (i < count + 3), False)
            weigh(p)
            total_up(1 - p)
            b, source = state[6:8]
            soften(b, source, p, False)
            wrap = source == 0
            more = i + 1 < count
            b_next = jnp.where(more, jnp.where(wrap, b + 1, b), b)
            next_source = jnp.where(more, jnp.where(wrap, b, source - 1), source)
            state = (*state[2:], b_next, next_source)
        return state

    if count > 0:
        lax.fori_loop(0, (count + 4) // 2, step, (jnp.int32(1), jnp.int32(0)) * 4)

    few = sub // 2
    keep = lax.broadcasted_iota(jnp.int32, (few, LANES), 1) < HEAD_DIM

    def finish(b, out_at):
        acc = acc_ref[b]
        turned = pltpu.roll(acc, HEAD_DIM, 1)
        for t in range(parts):
            left = turned[t * sub : t * sub + few]
            right = acc[t * sub + few : (t + 1) * sub]
            out_at[t] = jnp.where(keep, left, right).astype(bf16)

    if len(out_refs) > 1:
        for k, ref in enumerate(out_refs):
            for side in range(TOPK):
                finish(lax.axis_index("ep") ^ (k * TOPK + side), ref.at[side])
    else:

        def each(b, _):
            finish(b, out_refs[0].at[b])
            return 0

        lax.fori_loop(0, blocks, each, 0)


def project_with(source, weights, out_ref, *, few, heads, sharers):
    low = lax.broadcasted_iota(jnp.int32, (few, LANES), 1) < HEAD_DIM
    total = None
    for m, w_ref in enumerate(weights):
        strips = []
        for s in range(sharers):
            firsts, seconds = [], []
            for h in range(0, heads, 2):
                a = source(m, h * sharers + s).astype(f32)
                b = source(m, (h + 1) * sharers + s).astype(f32)
                firsts.append(jnp.where(low, a, pltpu.roll(b, HEAD_DIM, 1)))
                seconds.append(jnp.where(low, pltpu.roll(a, HEAD_DIM, 1), b))
            strips.append(jnp.concatenate(firsts, axis=1))
            strips.append(jnp.concatenate(seconds, axis=1))
        left = jnp.concatenate(strips, axis=0).astype(bf16)
        part = mm(left, w_ref[...])
        total = part if total is None else total + part
    out_ref[...] = total.astype(bf16)


def project_body(got_ref, *refs, heads, sharers, parts):
    here = lax.axis_index("tp")
    project_with(
        lambda m, ep: got_ref[ep * parts + (here ^ m)],
        refs[:-1],
        refs[-1],
        few=got_ref.shape[1],
        heads=heads,
        sharers=sharers,
    )


def sides_body(*refs):
    sources, (kept, given) = refs[:GROUPS], refs[GROUPS:]
    for k, source in enumerate(sources):
        kept[k] = source[0]
        given[k] = source[1]


def parts_body(kept, given, *outs):
    here = lax.axis_index("tp")
    for m, out in enumerate(outs):
        for k in range(GROUPS):
            for side, source in enumerate((kept, given)):
                out[k * TOPK + side] = source[k, here ^ m]


def project_pair_body(*refs, heads):
    here = lax.axis_index("ep")
    sources = refs[:4]
    project_with(
        lambda m, ep: sources[m][here ^ ep],
        refs[4:8],
        refs[8],
        few=sources[0].shape[1],
        heads=heads,
        sharers=TOPK,
    )


def stage_body(*refs):
    half = len(refs) // 2
    for a, b in zip(refs[:half], refs[half:]):
        b[...] = a[...]


def spread(piece, size):
    cross = [(i, i ^ 2) for i in range(size)]
    beside = [(i, i ^ 1) for i in range(size)]
    far = lax.ppermute(piece, "tp", cross)
    near = lax.ppermute(piece, "tp", beside)
    return (piece, near, far, lax.ppermute(far, "tp", beside))


def mixer(query_rows, key_rows, value_rows, key_bias, out_pieces, paired):
    rows = query_rows.shape[0]
    heads = query_rows.shape[1] // HEAD_DIM
    ep_count = lax.axis_size("ep")
    parts = lax.axis_size("tp")
    sharers = ep_count // heads
    sub = rows // parts // sharers
    mine = sub * parts
    tall = rows + mine // 2
    bias_type = jax.ShapeDtypeStruct((key_bias.shape[0] // KEY_TILE, KEY_TILE), f32)
    attend_type = jax.ShapeDtypeStruct((ep_count, parts, sub // 2, LANES), bf16)
    work = 3 * ep_count * ep_count * mine * rows * LANES
    scratch = [
        pltpu.VMEM((ep_count, mine, LANES), f32),
        pltpu.VMEM((ep_count, mine, LANES), f32),
        pltpu.VMEM((2, mine, rows), f32),
        pltpu.VMEM((2, mine, rows), f32),
        pltpu.VMEM((2, mine, rows), bf16),
        pltpu.VMEM((2, mine, rows), bf16),
        pltpu.VMEM((2, mine, LANES), f32),
        pltpu.VMEM((2, mine, LANES), f32),
    ]
    sizes = {"rows": rows, "sub": sub, "parts": parts}
    if paired:
        bias, *packed = call(
            functools.partial(pack_pair_body, heads=heads, parts=parts),
            [bias_type] + [jax.ShapeDtypeStruct((tall + mine // 2, LANES), bf16)] * GROUPS,
            [whole(key_bias.T)] + [whole(query_rows)] * 3,
            12,
            scratch=[pltpu.VMEM((heads, tall + mine // 2, LANES), bf16)],
        )(key_bias.T, query_rows, key_rows, value_rows)
        own = [packed[0]]
        for k in range(1, GROUPS):
            pairs = [(i, i ^ (k * TOPK)) for i in range(ep_count)]
            own.append(lax.ppermute(packed[k], "ep", pairs))
        across = [(i, i ^ 1) for i in range(ep_count)]
        theirs = [lax.ppermute(piece, "ep", across) for piece in own]
        block = (parts, sub // 2, LANES)
        attended = call(
            functools.partial(attend_pair_body, **sizes),
            [jax.ShapeDtypeStruct((TOPK, *block), bf16)] * GROUPS,
            [VMEM] * (1 + 2 * GROUPS),
            16,
            flops=work,
            scratch=[pltpu.VMEM((ep_count, tall, LANES), bf16)] + scratch,
        )(bias, *own, *theirs)
        attended = list(attended)
        for k in range(1, GROUPS):
            pairs = [(i, i ^ (k * TOPK)) for i in range(ep_count)]
            attended[k] = lax.ppermute(attended[k], "ep", pairs)
        side_type = jax.ShapeDtypeStruct((GROUPS, *block), bf16)
        kept, given = call(sides_body, [side_type] * 2, [VMEM] * GROUPS, 4)(*attended)
        given = lax.ppermute(given, "ep", across)
        by_part = call(
            parts_body,
            [jax.ShapeDtypeStruct((ep_count, sub // 2, LANES), bf16)] * parts,
            [VMEM] * 2,
            4,
        )(kept, given)
        by_part = list(by_part)
        for m in range(1, parts):
            pairs = [(i, i ^ m) for i in range(parts)]
            by_part[m] = lax.ppermute(by_part[m], "tp", pairs)
        return call(
            functools.partial(project_pair_body, heads=heads),
            jax.ShapeDtypeStruct((rows // parts, out_pieces[0].shape[1]), bf16),
            [VMEM] * 8,
            12,
            flops=2 * rows * heads * HEAD_DIM * out_pieces[0].shape[1],
        )(*by_part, *out_pieces)
    else:
        bias, outgoing = call(
            functools.partial(pack_body, heads=heads, sharers=sharers, parts=parts),
            [bias_type, jax.ShapeDtypeStruct((ep_count, tall, LANES), bf16)],
            [whole(key_bias.T)] + [whole(query_rows)] * 3,
            12,
        )(key_bias.T, query_rows, key_rows, value_rows)
        got = exchange(outgoing, "ep")
        attended = call(
            functools.partial(attend_body, **sizes),
            attend_type,
            [VMEM, VMEM],
            16,
            flops=work,
            scratch=scratch,
        )(got, bias)
    attended = attended.reshape(ep_count * parts, sub // 2, LANES)
    back = exchange(attended, ("ep", "tp"))
    return call(
        functools.partial(project_body, heads=heads, sharers=sharers, parts=parts),
        jax.ShapeDtypeStruct((rows // parts, out_pieces[0].shape[1]), bf16),
        [VMEM] * 5,
        12,
        flops=2 * rows * heads * HEAD_DIM * out_pieces[0].shape[1],
    )(back, *out_pieces)


def route_body(x_ref, gain_ref, pick_ref, weight_ref, *outs, cap):
    out_refs, turn_ref = outs[:GROUPS], outs[GROUPS]
    tokens, width = x_ref.shape
    z = spot_of(TOPK)[2]
    pick = pick_ref[...]
    lanes = GROUPS * 2
    group = lax.broadcasted_iota(jnp.int32, (lanes, tokens), 0)
    inside = (pick[0:1] >= group * TOPK) & (pick[0:1] < (group + 1) * TOPK)
    match = jnp.where(inside, 1.0, 0.0)
    before = (
        lax.broadcasted_iota(jnp.int32, (tokens, tokens), 0)
        < lax.broadcasted_iota(jnp.int32, (tokens, tokens), 1)
    )
    rank = mm(match.astype(bf16), jnp.where(before, 1.0, 0.0).astype(bf16))
    first = ((group ^ z) * cap).astype(f32)
    slot = jnp.sum(match * (rank + first), axis=0, keepdims=True).astype(jnp.int32)
    place = lax.broadcasted_iota(jnp.int32, (GROUPS * cap, tokens), 0) == slot
    place = jnp.where(place, 1.0, 0.0)
    weight = weight_ref[...]
    odd = (pick & 1) == 1
    one = jnp.sum(jnp.where(odd, weight, 0.0), axis=0, keepdims=True)
    zero = jnp.sum(jnp.where(odd, 0.0, weight), axis=0, keepdims=True)
    line = lax.broadcasted_iota(jnp.int32, (LANES, tokens), 0)
    value = jnp.where((line & 1) == 1, one, zero)
    high = value.astype(bf16).astype(f32)
    extra = jnp.where(line < 2, high, value - high).astype(bf16)
    place_b = place.astype(bf16)
    turn_ref[...] = place.T.astype(bf16)
    wide = x_ref[...].astype(f32)
    normed = (
        wide
        * lax.rsqrt(jnp.mean(wide * wide, axis=1, keepdims=True) + norm_eps)
        * gain_ref[...]
    ).astype(bf16)
    for k, ref in enumerate(out_refs):
        strip = place_b[k * cap : (k + 1) * cap]
        ref[:, :width] = mm(strip, normed).astype(bf16)
        ref[:, width:] = lax.dot_general(
            strip, extra, (((1,), (1,)), ((), ())), preferred_element_type=f32
        ).astype(bf16)


def expand_body(*refs):
    rows, gates, ups = refs[:GROUPS], refs[GROUPS : GROUPS + 4], refs[GROUPS + 4 : GROUPS + 8]
    out_ref, mix_ref = refs[GROUPS + 8 :]
    width, part = gates[0].shape
    x = jnp.concatenate([r[:, :width] for r in rows], axis=0)
    mix_ref[...] = jnp.concatenate([r[:, width:] for r in rows], axis=0)
    for i in range(4):
        gate = mm(x, gates[i][...])
        up = mm(x, ups[i][...])
        out_ref[:, i * part : (i + 1) * part] = (gate / (1.0 + jnp.exp(-gate)) * up).astype(bf16)


def contract_body(h_ref, d0, d1, d2, d3, *out_refs):
    cap = out_refs[0].shape[0]
    part = d0.shape[0]
    total = None
    for i, d in enumerate((d0, d1, d2, d3)):
        got = mm(h_ref[:, i * part : (i + 1) * part], d[...])
        total = got if total is None else total + got
    for k, ref in enumerate(out_refs):
        ref[...] = total[k * cap : (k + 1) * cap].astype(bf16)


def join_body(own_ref, other_ref, mix_ref, out_ref, *, first):
    extra = mix_ref[first : first + own_ref.shape[0]].astype(f32)
    zero = extra[:, 0:1] + extra[:, 2:3]
    one = extra[:, 1:2] + extra[:, 3:4]
    odd = spot_of(TOPK)[0] == 1
    mine = jnp.where(odd, one, zero)
    theirs = jnp.where(odd, zero, one)
    out_ref[...] = (own_ref[...].astype(f32) * mine + other_ref[...].astype(f32) * theirs).astype(bf16)


def restore_body(turn_ref, *refs):
    out_ref = refs[-1]
    cap = refs[0].shape[0]
    total = None
    for k, ref in enumerate(refs[:-1]):
        got = mm(turn_ref[:, k * cap : (k + 1) * cap], ref[...])
        total = got if total is None else total + got
    out_ref[...] = total.astype(bf16)


def paired_experts(moe_input, moe_gain, expert_pick, route_weight, gates, ups, downs):
    tokens, width = moe_input.shape
    ep_count = lax.axis_size("ep")
    cap = GROUPS * tokens // ep_count

    def along(k):
        return [(i, i ^ (k * TOPK)) for i in range(ep_count)]

    across = [(i, i ^ 1) for i in range(ep_count)]
    row_type = jax.ShapeDtypeStruct((cap, width + LANES), bf16)
    wide_type = jax.ShapeDtypeStruct((cap, width), bf16)
    route_args = (moe_input, moe_gain.reshape(1, width), expert_pick.T, route_weight.T)
    *sent, turn = call(
        functools.partial(route_body, cap=cap),
        [row_type] * GROUPS + [jax.ShapeDtypeStruct((tokens, GROUPS * cap), bf16)],
        [whole(a) for a in route_args],
        12,
    )(*route_args)
    own = [sent[0]] + [lax.ppermute(sent[k], "ep", along(k)) for k in range(1, GROUPS)]
    theirs = [lax.ppermute(rows, "ep", across) for rows in own]
    part = gates[0].shape[2]
    count = GROUPS * cap
    gates = [g[0] for g in gates]
    ups = [u[0] for u in ups]
    piece_type = jax.ShapeDtypeStruct(gates[0].shape, bf16)
    gates[0], ups[0] = call(stage_body, [piece_type] * 2, [VMEM] * 2, 8)(gates[0], ups[0])
    results = {}
    for side, rows in (("a", own), ("b", theirs)):
        hidden, got = call(
            expand_body,
            [
                jax.ShapeDtypeStruct((count, 4 * part), bf16),
                jax.ShapeDtypeStruct((count, LANES), bf16),
            ],
            [VMEM] * (GROUPS + 8),
            16,
            flops=4 * count * width * 4 * part,
        )(*rows, *gates, *ups)
        if side == "a":
            mix = got
        results[side] = call(
            contract_body, [wide_type] * GROUPS, [VMEM] * 5, 16, flops=2 * count * width * 4 * part
        )(hidden, *[d[0] for d in downs])
    others = [None] * GROUPS
    returned = [None] * GROUPS
    for k in RETURN_ORDER:
        others[k] = lax.ppermute(results["b"][k], "ep", across)
    for k in RETURN_ORDER:
        joined = call(
            functools.partial(join_body, first=k * cap), wide_type, [VMEM] * 3, 4
        )(results["a"][k], others[k], mix)
        returned[k] = lax.ppermute(joined, "ep", along(k)) if k else joined
    return call(
        restore_body, jax.ShapeDtypeStruct((tokens, width), bf16), [VMEM] * (GROUPS + 1), 8
    )(turn, *returned)


def expand(arrived, gate_weights, up_weights):
    gate_in = jnp.einsum("necm,emf->necf", arrived, gate_weights, preferred_element_type=f32)
    up_in = jnp.einsum("necm,emf->necf", arrived, up_weights, preferred_element_type=f32)
    return (jax.nn.silu(gate_in) * up_in).astype(bf16)


def contract(hidden, down_weights):
    return jnp.einsum("necf,efm->necm", hidden, down_weights, preferred_element_type=f32)


def any_experts(moe_input, moe_gain, expert_pick, route_weight, w_gate, w_up, w_down):
    ep_count = lax.axis_size("ep")
    token_count = moe_input.shape[0]
    widened = moe_input.astype(f32)
    normed = (
        widened
        * lax.rsqrt(jnp.mean(widened * widened, axis=1, keepdims=True) + norm_eps)
        * moe_gain
    ).astype(bf16)
    local_experts = w_gate.shape[0]
    expert_total = local_experts * ep_count
    capacity = GROUPS * token_count // expert_total
    picks = expert_pick.reshape(-1)
    matches = (picks[:, None] == jnp.arange(expert_total, dtype=jnp.int32)[None, :]).astype(
        jnp.int32
    )
    ranks = jnp.sum((jnp.cumsum(matches, axis=0) - matches) * matches, axis=1)
    slots = picks * capacity + ranks
    owners = jnp.arange(picks.shape[0], dtype=jnp.int32) // TOPK
    table = jnp.full((expert_total * capacity,), token_count, jnp.int32).at[slots].set(owners)
    padded = jnp.concatenate([normed, jnp.zeros((1, normed.shape[1]), bf16)], axis=0)
    outgoing = padded[table].reshape(ep_count, local_experts, capacity, normed.shape[1])
    arrived = lax.all_to_all(outgoing, "ep", split_axis=0, concat_axis=0, tiled=True)
    gate_all, up_all, down_all = (
        lax.all_gather(w_gate, "tp", axis=2, tiled=True),
        lax.all_gather(w_up, "tp", axis=2, tiled=True),
        lax.all_gather(w_down, "tp", axis=1, tiled=True),
    )
    served = contract(expand(arrived, gate_all, up_all), down_all).astype(bf16)
    returned = lax.all_to_all(served, "ep", split_axis=0, concat_axis=0, tiled=True)
    flat = returned.reshape(expert_total * capacity, returned.shape[3])
    chosen = flat[slots].reshape(token_count, TOPK, flat.shape[1]).astype(f32)
    return jnp.sum(chosen * route_weight[:, :, None], axis=1).astype(bf16)


def local(
    query_rows,
    key_rows,
    value_rows,
    key_bias,
    out_weight,
    moe_input,
    moe_gain,
    expert_pick,
    route_weight,
    w_gate,
    w_up,
    w_down,
):
    tp_size = lax.axis_size("tp")
    paired = is_paired(lax.axis_size("ep"), w_gate.shape[0])
    paired = paired and query_rows.shape[1] == GROUPS * HEAD_DIM
    if paired:
        gates = spread(w_gate, tp_size)
        ups = spread(w_up, tp_size)
        downs = spread(w_down, tp_size)
        routed_out = paired_experts(
            moe_input, moe_gain, expert_pick, route_weight, gates, ups, downs
        )
    else:
        routed_out = any_experts(
            moe_input, moe_gain, expert_pick, route_weight, w_gate, w_up, w_down
        )
    out_pieces = spread(out_weight, tp_size)
    mixer_out = mixer(query_rows, key_rows, value_rows, key_bias, out_pieces, paired)
    return (mixer_out, routed_out)


def is_paired(ep_count, local_experts):
    return local_experts == 1 and ep_count == GROUPS * TOPK


def solution(mesh):
    placed = (
        P("ep", "tp"),
        P("ep", "tp"),
        P("ep", "tp"),
        P(None, "tp"),
        P("tp", None),
        P(("ep", "tp"), None),
        P(),
        P(("ep", "tp"), None),
        P(("ep", "tp"), None),
        P("ep", None, "tp"),
        P("ep", None, "tp"),
        P("ep", "tp", None),
    )
    return jax.shard_map(
        local,
        mesh=mesh,
        in_specs=placed,
        out_specs=(P(("ep", "tp"), None), P(("ep", "tp"), None)),
        check_vma=False,
    )
```

time: 191 us -> 179 us (0.937)
  waiting for transfers between devices: 65.7 us -> 94.9 us
  Pallas kernels: 56.8 us -> 31.2 us
  local copies, waits for them, and re-layouts: 27.9 us -> 6.88 us
  starting transfers between devices: 37.2 us -> 45 us
    pallas_call x12 -> x16, Pallas kernels: 56.8 us -> 31.2 us  [the longest x1 18 us: mixer(): call(functools.partial(attend_pair_body, **sizes), [jax.ShapeDtypeStruct(...]
    ppermute x4, waiting for transfers between devices: 25.7 us -> 47 us  [spread(): far = lax.ppermute(piece, 'tp', cross)]
    ppermute x4 -> x18, starting transfers between devices: 3.06 us -> 24.2 us  [the longest x3 6.99 us: mixer(): attended[k] = lax.ppermute(attended[k], 'ep', pairs)]
    unnamed x72 -> x24, local copies, waits for them, and re-layouts: 27.9 us -> 6.88 us
    ppermute x4 -> x18, waiting for transfers between devices: 3.31 us -> 24.2 us  [the longest x4 14.3 us: paired_experts(): others[k] = lax.ppermute(results['b'][k], 'ep', across)]
    ppermute x3, waiting for transfers between devices: 14.9 us -> 0.01 us  [paired_experts(): lax.ppermute(sent[k], 'ep', along(k))]
    all_to_all x2 -> x0, starting transfers between devices: 11.8 us -> none  [the longest x1 6.98 us: mixer(): lax.all_to_all(outgoing, 'ep', split_axis=0, concat_axis=0, tiled=True)]
    ppermute x3, waiting for transfers between devices: 16 us -> 18 us  [paired_experts(): returned[k] = lax.ppermute(joined, 'ep', along(k)) if k else joined]
  transfers between devices with their start and end apart: 28 -> 40, of which waited for: 11 -> 13; matrix products, arithmetic and copies ran while one was open for 1% -> 0% of each run, Pallas kernels for 27% -> 16%
where the time goes in v2:
time: 179 us
  waiting for transfers between devices  94.9 us (53%)
  starting transfers between devices  45 us (25%)
  Pallas kernels  31.2 us (17%)
  local copies, waits for them, and re-layouts  6.88 us (4%)
    ppermute x4, waiting for transfers between devices, spread(): far = lax.ppermute(piece, 'tp', cross)  47 us
    ppermute x3, waiting for transfers between devices, paired_experts(): returned[k] = lax.ppermute(joined, 'ep', along(k)) if k else joined  18 us
    pallas_call x1, Pallas kernels, mixer(): call(functools.partial(attend_pair_body, **sizes), [jax.ShapeDtypeStruct(...  18 us
    ppermute x4, waiting for transfers between devices, paired_experts(): others[k] = lax.ppermute(results['b'][k], 'ep', across)  14.3 us
    ppermute x3, starting transfers between devices, mixer(): attended[k] = lax.ppermute(attended[k], 'ep', pairs)  6.99 us
    ppermute x3, waiting for transfers between devices, mixer(): own.append(lax.ppermute(packed[k], 'ep', pairs))  6.88 us
    unnamed x24, local copies, waits for them, and re-layouts  6.88 us
    ppermute x3, starting transfers between devices, paired_experts(): lax.ppermute(sent[k], 'ep', along(k))  6.21 us
  transfers between devices with their start and end apart: 40, of which 13 were waited for; matrix products, arithmetic and copies ran while one was open for 0% of the time, Pallas kernels for 16%

profile of v2, /device:TPU:0, one launch (start us, length us, event | category | flops | bytes accessed | tf_op | source)
XLA Modules:
  0.0 178.8 jit_solution(16907847163174170162)
XLA Ops:
  4.7 3.1 %collective-permute-start = (bf16[768,128]{1,0:T(8,128)(2,1)S(1)}, bf16[768,128]{1,0:T(8,128)(2,1)S(1)}, u32[]{:S(2)}, u32[]{:S(2)}) collective-permute-start(bf16[768,128]{1,0:T(8,128)(2,1)S(1)} %get-tuple-element.37), channel_id=1, source_target_pairs={{0,8},{4,12},{8,0},{12,4},{16,24},{20,28},{24,16},{28,20},{1,9},{5... | collective-permute-start | bytes 589832 | tf_op jit(solution)/shard_map/ppermute | solution.py:370
  7.9 2.6 %collective-permute-start.1 = (bf16[768,128]{1,0:T(8,128)(2,1)S(1)}, bf16[768,128]{1,0:T(8,128)(2,1)S(1)}, u32[]{:S(2)}, u32[]{:S(2)}) collective-permute-start(bf16[768,128]{1,0:T(8,128)(2,1)S(1)} %get-tuple-element.38), channel_id=1, source_target_pairs={{0,16},{4,20},{8,24},{12,28},{16,0},{20,4},{24,8},{28,12},{1,17},{... | collective-permute-start | bytes 589832 | tf_op jit(solution)/shard_map/ppermute | solution.py:370
  18.1 6.9 %collective-permute-done.1.refs_2_ = bf16[768,128]{1,0:T(8,128)(2,1)S(1)} collective-permute-done((bf16[768,128]{1,0:T(8,128)(2,1)S(1)}, bf16[768,128]{1,0:T(8,128)(2,1)S(1)}, u32[]{:S(2)}, u32[]{:S(2)}) %collective-permute-start.1) | collective-permute-done | bytes 196640 | tf_op jit(solution)/shard_map/ppermute | solution.py:370
  27.0 3.9 %collective-permute-start.18 = (bf16[64,2176]{1,0:T(8,128)(2,1)S(1)}, bf16[64,2176]{1,0:T(8,128)(2,1)S(1)}, u32[]{:S(2)}, u32[]{:S(2)}) collective-permute-start(bf16[64,2176]{1,0:T(8,128)(2,1)S(1)} %get-tuple-element.53), channel_id=1, source_target_pairs={{0,16},{4,20},{8,24},{12,28},{16,0},{20,4},{24,8},{28,12},{1,17},{... | collective-permute-start | bytes 835592 | tf_op jit(solution)/shard_map/ppermute | solution.py:536
  33.8 2.6 %collective-permute-start.29 = (bf16[64,2176]{1,0:T(8,128)(2,1)S(1)}, bf16[64,2176]{1,0:T(8,128)(2,1)S(1)}, u32[]{:S(2)}, u32[]{:S(2)}) collective-permute-start(bf16[64,2176]{1,0:T(8,128)(2,1)S(1)} %get-tuple-element.51.refs_0_), channel_id=1, source_target_pairs={{0,4},{4,0},{8,12},{12,8},{16,20},{20,16},{24,28},{28,24},{1,5},{5... | collective-permute-start | bytes 835592 | tf_op jit(solution)/shard_map/ppermute | solution.py:537
  36.4 18.0 %shard_map.132 = (bf16[2,4,32,128]{3,2,1,0:T(8,128)(2,1)S(1)}, bf16[2,4,32,128]{3,2,1,0:T(8,128)(2,1)S(1)}, bf16[2,4,32,128]{3,2,1,0:T(8,128)(2,1)S(1)}, bf16[2,4,32,128]{3,2,1,0:T(8,128)(2,1)S(1)}) custom-call(f32[16,256]{1,0:T(8,128)S(1)} %get-tuple-element.35.bias_ref, bf16[768,128]{1,0:T(8,128)(2,1)S(1)} %get-tuple-element.36.refs_0_, ...), custom_call_target="tpu_custom_call" | custom-call | flops 3221225472 | tf_op jit(solution)/shard_map/pallas_call | solution.py:374
  57.3 3.1 %collective-permute-start.8 = (bf16[2,4,32,128]{3,2,1,0:T(8,128)(2,1)S(1)}, bf16[2,4,32,128]{3,2,1,0:T(8,128)(2,1)S(1)}, u32[]{:S(2)}, u32[]{:S(2)}) collective-permute-start(bf16[2,4,32,128]{3,2,1,0:T(8,128)(2,1)S(1)} %get-tuple-element.42), channel_id=1, source_target_pairs={{0,16},{4,20},{8,24},{12,28},{16,0},{20,4},{24,8},{28,12},{1,17},{... | collective-permute-start | bytes 196616 | tf_op jit(solution)/shard_map/ppermute | solution.py:385
  60.4 2.5 %collective-permute-start.9 = (bf16[2,4,32,128]{3,2,1,0:T(8,128)(2,1)S(1)}, bf16[2,4,32,128]{3,2,1,0:T(8,128)(2,1)S(1)}, u32[]{:S(2)}, u32[]{:S(2)}) collective-permute-start(bf16[2,4,32,128]{3,2,1,0:T(8,128)(2,1)S(1)} %get-tuple-element.43), channel_id=1, source_target_pairs={{0,24},{4,28},{8,16},{12,20},{16,8},{20,12},{24,0},{28,4},{1,25},{... | collective-permute-start | bytes 196616 | tf_op jit(solution)/shard_map/ppermute | solution.py:385
  63.4 3.1 %collective-permute-done.9.refs_3_ = bf16[2,4,32,128]{3,2,1,0:T(8,128)(2,1)S(1)} collective-permute-done((bf16[2,4,32,128]{3,2,1,0:T(8,128)(2,1)S(1)}, bf16[2,4,32,128]{3,2,1,0:T(8,128)(2,1)S(1)}, u32[]{:S(2)}, u32[]{:S(2)}) %collective-permute-start.9) | collective-permute-done | bytes 65568 | tf_op jit(solution)/shard_map/ppermute | solution.py:385
  67.5 2.5 %collective-permute-done.31.refs_2_ = bf16[64,2176]{1,0:T(8,128)(2,1)S(1)} collective-permute-done((bf16[64,2176]{1,0:T(8,128)(2,1)S(1)}, bf16[64,2176]{1,0:T(8,128)(2,1)S(1)}, u32[]{:S(2)}, u32[]{:S(2)}) %collective-permute-start.31) | collective-permute-done | bytes 278560 | tf_op jit(solution)/shard_map/ppermute | solution.py:537
  70.0 3.0 %collective-permute-done.32.refs_3_ = bf16[64,2176]{1,0:T(8,128)(2,1)S(1)} collective-permute-done((bf16[64,2176]{1,0:T(8,128)(2,1)S(1)}, bf16[64,2176]{1,0:T(8,128)(2,1)S(1)}, u32[]{:S(2)}, u32[]{:S(2)}) %collective-permute-start.32) | collective-permute-done | bytes 278560 | tf_op jit(solution)/shard_map/ppermute | solution.py:537
  75.1 6.7 %collective-permute-done.21 = bf16[1,2048,256]{2,1,0:T(8,128)(2,1)S(1)} collective-permute-done((bf16[1,2048,256]{2,1,0:T(8,128)(2,1)S(1)}, bf16[1,2048,256]{2,1,0:T(8,128)(2,1)S(1)}, u32[]{:S(2)}, u32[]{:S(2)}) %collective-permute-start.21) | collective-permute-done | bytes 1048608 | tf_op jit(solution)/shard_map/ppermute | solution.py:331
  82.4 21.9 %collective-permute-done.27 = bf16[1,256,2048]{2,1,0:T(8,128)(2,1)S(1)} collective-permute-done((bf16[1,256,2048]{2,1,0:T(8,128)(2,1)S(1)}, bf16[1,256,2048]{2,1,0:T(8,128)(2,1)S(1)}, u32[]{:S(2)}, u32[]{:S(2)}) %collective-permute-start.27) | collective-permute-done | bytes 1048608 | tf_op jit(solution)/shard_map/ppermute | solution.py:331
  104.3 18.4 %collective-permute-done.15.refs_6_ = bf16[256,2048]{1,0:T(8,128)(2,1)S(1)} collective-permute-done((bf16[256,2048]{1,0:T(8,128)(2,1)S(1)}, bf16[256,2048]{1,0:T(8,128)(2,1)S(1)}, u32[]{:S(2)}, u32[]{:S(2)}) %collective-permute-start.15) | collective-permute-done | bytes 1048608 | tf_op jit(solution)/shard_map/ppermute | solution.py:331
  124.7 2.9 %shard_map.140 = (bf16[256,1024]{1,0:T(8,128)(2,1)S(1)}, bf16[256,128]{1,0:T(8,128)(2,1)}) custom-call(bf16[64,2176]{1,0:T(8,128)(2,1)S(1)} %collective-permute-done.29.refs_0_, bf16[64,2176]{1,0:T(8,128)(2,1)S(1)} %collective-permute-done.30.refs_1_, bf16[64,2176]{1,0:T(8,128)(2,1)S(1)} %collective-permute-done.31.refs_2_, ...), custom_call_target="tpu_custom_call" | custom-call | flops 2147483648 | tf_op jit(solution)/shard_map/pallas_call | solution.py:546
  131.8 2.4 %shard_map.138 = (bf16[256,1024]{1,0:T(8,128)(2,1)S(1)}, bf16[256,128]{1,0:T(8,128)(2,1)S(1)}) custom-call(bf16[64,2176]{1,0:T(8,128)(2,1)S(1)} %get-tuple-element.51.refs_0_, bf16[64,2176]{1,0:T(8,128)(2,1)S(1)} %collective-permute-done.17.refs_1_, bf16[64,2176]{1,0:T(8,128)(2,1)S(1)} %collective-permute-done.18.refs_2_, ...), custom_call_target="tpu_custom_call" | custom-call | flops 2147483648 | tf_op jit(solution)/shard_map/pallas_call | solution.py:546
  134.2 4.0 %collective-permute-done.38.other_ref = bf16[64,2048]{1,0:T(8,128)(2,1)S(1)} collective-permute-done((bf16[64,2048]{1,0:T(8,128)(2,1)S(1)}, bf16[64,2048]{1,0:T(8,128)(2,1)S(1)}, u32[]{:S(2)}, u32[]{:S(2)}) %collective-permute-start.38) | collective-permute-done | bytes 262176 | tf_op jit(solution)/shard_map/ppermute | solution.py:564
  138.1 5.6 %collective-permute-done.36.other_ref = bf16[64,2048]{1,0:T(8,128)(2,1)S(1)} collective-permute-done((bf16[64,2048]{1,0:T(8,128)(2,1)S(1)}, bf16[64,2048]{1,0:T(8,128)(2,1)S(1)}, u32[]{:S(2)}, u32[]{:S(2)}) %collective-permute-start.36) | collective-permute-done | bytes 262176 | tf_op jit(solution)/shard_map/ppermute | solution.py:564
  145.2 2.9 %collective-permute-done.34.other_ref = bf16[64,2048]{1,0:T(8,128)(2,1)S(1)} collective-permute-done((bf16[64,2048]{1,0:T(8,128)(2,1)S(1)}, bf16[64,2048]{1,0:T(8,128)(2,1)S(1)}, u32[]{:S(2)}, u32[]{:S(2)}) %collective-permute-start.34) | collective-permute-done | bytes 262176 | tf_op jit(solution)/shard_map/ppermute | solution.py:564
  151.2 2.9 %collective-permute-start.39 = (bf16[64,2048]{1,0:T(8,128)(2,1)S(1)}, bf16[64,2048]{1,0:T(8,128)(2,1)S(1)}, u32[]{:S(2)}, u32[]{:S(2)}) collective-permute-start(bf16[64,2048]{1,0:T(8,128)(2,1)S(1)} %shard_map.145), channel_id=1, source_target_pairs={{0,24},{4,28},{8,16},{12,20},{16,8},{20,12},{24,0},{28,4},{1,25},{... | collective-permute-start | bytes 786440 | tf_op jit(solution)/shard_map/ppermute | solution.py:569
  155.6 1.6 shard_map.135
  157.1 1.8 collective-permute-done.33.other_ref
  159.2 2.8 %collective-permute-done.39.refs_3_ = bf16[64,2048]{1,0:T(8,128)(2,1)S(1)} collective-permute-done((bf16[64,2048]{1,0:T(8,128)(2,1)S(1)}, bf16[64,2048]{1,0:T(8,128)(2,1)S(1)}, u32[]{:S(2)}, u32[]{:S(2)}) %collective-permute-start.39) | collective-permute-done | bytes 262176 | tf_op jit(solution)/shard_map/ppermute | solution.py:569
  162.0 15.3 %collective-permute-done.37.refs_2_ = bf16[64,2048]{1,0:T(8,128)(2,1)S(1)} collective-permute-done((bf16[64,2048]{1,0:T(8,128)(2,1)S(1)}, bf16[64,2048]{1,0:T(8,128)(2,1)S(1)}, u32[]{:S(2)}, u32[]{:S(2)}) %collective-permute-start.37) | collective-permute-done | bytes 262176 | tf_op jit(solution)/shard_map/ppermute | solution.py:569
  (96 shorter events, 37.7 us)
Async XLA Ops:
  7.9 17.1 %collective-permute-start.1 = (bf16[768,128]{1,0:T(8,128)(2,1)S(1)}, bf16[768,128]{1,0:T(8,128)(2,1)S(1)}, u32[]{:S(2)}, u32[]{:S(2)}) collective-permute-start(bf16[768,128]{1,0:T(8,128)(2,1)S(1)} %get-tuple-element.38), channel_id=1, source_target_pairs={{0,16},{4,20},{8,24},{12,28},{16,0},{20,4},{24,8},{28,12},{1,17},{... | collective-permute-start | bytes 589832 | tf_op jit(solution)/shard_map/ppermute | solution.py:370
  10.5 16.1 %collective-permute-start.2 = (bf16[768,128]{1,0:T(8,128)(2,1)S(1)}, bf16[768,128]{1,0:T(8,128)(2,1)S(1)}, u32[]{:S(2)}, u32[]{:S(2)}) collective-permute-start(bf16[768,128]{1,0:T(8,128)(2,1)S(1)} %get-tuple-element.39), channel_id=1, source_target_pairs={{0,24},{4,28},{8,16},{12,20},{16,8},{20,12},{24,0},{28,4},{1,25},{... | collective-permute-start | bytes 589832 | tf_op jit(solution)/shard_map/ppermute | solution.py:370
  14.3 16.7 %collective-permute-start.17 = (bf16[64,2176]{1,0:T(8,128)(2,1)S(1)}, bf16[64,2176]{1,0:T(8,128)(2,1)S(1)}, u32[]{:S(2)}, u32[]{:S(2)}) collective-permute-start(bf16[64,2176]{1,0:T(8,128)(2,1)S(1)} %get-tuple-element.52), channel_id=1, source_target_pairs={{0,8},{4,12},{8,0},{12,4},{16,24},{20,28},{24,16},{28,20},{1,9},{5... | collective-permute-start | bytes 835592 | tf_op jit(solution)/shard_map/ppermute | solution.py:536
  16.7 15.6 %collective-permute-start.4 = (bf16[768,128]{1,0:T(8,128)(2,1)S(1)}, bf16[768,128]{1,0:T(8,128)(2,1)S(1)}, u32[]{:S(2)}, u32[]{:S(2)}) collective-permute-start(bf16[768,128]{1,0:T(8,128)(2,1)S(1)} %collective-permute-done.refs_1_), channel_id=1, source_target_pairs={{0,4},{4,0},{8,12},{12,8},{16,20},{20,16},{24,28},{28,24},{1,5},{5... | collective-permute-start | bytes 589832 | tf_op jit(solution)/shard_map/ppermute | solution.py:372
  27.0 27.4 %collective-permute-start.18 = (bf16[64,2176]{1,0:T(8,128)(2,1)S(1)}, bf16[64,2176]{1,0:T(8,128)(2,1)S(1)}, u32[]{:S(2)}, u32[]{:S(2)}) collective-permute-start(bf16[64,2176]{1,0:T(8,128)(2,1)S(1)} %get-tuple-element.53), channel_id=1, source_target_pairs={{0,16},{4,20},{8,24},{12,28},{16,0},{20,4},{24,8},{28,12},{1,17},{... | collective-permute-start | bytes 835592 | tf_op jit(solution)/shard_map/ppermute | solution.py:536
  31.0 24.8 %collective-permute-start.19 = (bf16[64,2176]{1,0:T(8,128)(2,1)S(1)}, bf16[64,2176]{1,0:T(8,128)(2,1)S(1)}, u32[]{:S(2)}, u32[]{:S(2)}) collective-permute-start(bf16[64,2176]{1,0:T(8,128)(2,1)S(1)} %get-tuple-element.54), channel_id=1, source_target_pairs={{0,24},{4,28},{8,16},{12,20},{16,8},{20,12},{24,0},{28,4},{1,25},{... | collective-permute-start | bytes 835592 | tf_op jit(solution)/shard_map/ppermute | solution.py:536
  32.3 42.0 %collective-permute-start.24 = (bf16[1,2048,256]{2,1,0:T(8,128)(2,1)S(1)}, bf16[1,2048,256]{2,1,0:T(8,128)(2,1)S(1)}, u32[]{:S(2)}, u32[]{:S(2)}) collective-permute-start(bf16[1,2048,256]{2,1,0:T(8,128)(2,1)S(1)} %copy-done.3), channel_id=1, source_target_pairs={{0,2},{1,3},{2,0},{3,1},{4,6},{5,7},{6,4},{7,5},{8,10},{9,11},{10,... | collective-permute-start | bytes 3145736 | tf_op jit(solution)/shard_map/ppermute | solution.py:331
  33.8 23.4 %collective-permute-start.29 = (bf16[64,2176]{1,0:T(8,128)(2,1)S(1)}, bf16[64,2176]{1,0:T(8,128)(2,1)S(1)}, u32[]{:S(2)}, u32[]{:S(2)}) collective-permute-start(bf16[64,2176]{1,0:T(8,128)(2,1)S(1)} %get-tuple-element.51.refs_0_), channel_id=1, source_target_pairs={{0,4},{4,0},{8,12},{12,8},{16,20},{20,16},{24,28},{28,24},{1,5},{5... | collective-permute-start | bytes 835592 | tf_op jit(solution)/shard_map/ppermute | solution.py:537
  36.4 31.1 %collective-permute-start.30 = (bf16[64,2176]{1,0:T(8,128)(2,1)S(1)}, bf16[64,2176]{1,0:T(8,128)(2,1)S(1)}, u32[]{:S(2)}, u32[]{:S(2)}) collective-permute-start(bf16[64,2176]{1,0:T(8,128)(2,1)S(1)} %collective-permute-done.17.refs_1_), channel_id=1, source_target_pairs={{0,4},{4,0},{8,12},{12,8},{16,20},{20,16},{24,28},{28,24},{1,5},{5... | collective-permute-start | bytes 835592 | tf_op jit(solution)/shard_map/ppermute | solution.py:537
  55.8 26.0 %collective-permute-start.21 = (bf16[1,2048,256]{2,1,0:T(8,128)(2,1)S(1)}, bf16[1,2048,256]{2,1,0:T(8,128)(2,1)S(1)}, u32[]{:S(2)}, u32[]{:S(2)}) collective-permute-start(bf16[1,2048,256]{2,1,0:T(8,128)(2,1)S(1)} %copy-done.2), channel_id=1, source_target_pairs={{0,2},{1,3},{2,0},{3,1},{4,6},{5,7},{6,4},{7,5},{8,10},{9,11},{10,... | collective-permute-start | bytes 3145736 | tf_op jit(solution)/shard_map/ppermute | solution.py:331
  67.5 14.3 %collective-permute-start.20 = (bf16[1,2048,256]{2,1,0:T(8,128)(2,1)S(1)}, bf16[1,2048,256]{2,1,0:T(8,128)(2,1)S(1)}, u32[]{:S(2)}, u32[]{:S(2)}) collective-permute-start(bf16[1,2048,256]{2,1,0:T(8,128)(2,1)S(1)} %copy-done.2), channel_id=1, source_target_pairs={{0,1},{1,0},{2,3},{3,2},{4,5},{5,4},{6,7},{7,6},{8,9},{9,8},{10,11... | collective-permute-start | bytes 3145736 | tf_op jit(solution)/shard_map/ppermute | solution.py:332
  70.0 12.3 %collective-permute-start.23 = (bf16[1,2048,256]{2,1,0:T(8,128)(2,1)S(1)}, bf16[1,2048,256]{2,1,0:T(8,128)(2,1)S(1)}, u32[]{:S(2)}, u32[]{:S(2)}) collective-permute-start(bf16[1,2048,256]{2,1,0:T(8,128)(2,1)S(1)} %copy-done.3), channel_id=1, source_target_pairs={{0,1},{1,0},{2,3},{3,2},{4,5},{5,4},{6,7},{7,6},{8,9},{9,8},{10,11... | collective-permute-start | bytes 3145736 | tf_op jit(solution)/shard_map/ppermute | solution.py:332
  73.0 31.2 %collective-permute-start.27 = (bf16[1,256,2048]{2,1,0:T(8,128)(2,1)S(1)}, bf16[1,256,2048]{2,1,0:T(8,128)(2,1)S(1)}, u32[]{:S(2)}, u32[]{:S(2)}) collective-permute-start(bf16[1,256,2048]{2,1,0:T(8,128)(2,1)S(1)} %copy-done), channel_id=1, source_target_pairs={{0,2},{1,3},{2,0},{3,1},{4,6},{5,7},{6,4},{7,5},{8,10},{9,11},{10,... | collective-permute-start | bytes 3145736 | tf_op jit(solution)/shard_map/ppermute | solution.py:331
  74.3 48.4 %collective-permute-start.15 = (bf16[256,2048]{1,0:T(8,128)(2,1)S(1)}, bf16[256,2048]{1,0:T(8,128)(2,1)S(1)}, u32[]{:S(2)}, u32[]{:S(2)}) collective-permute-start(bf16[256,2048]{1,0:T(8,128)(2,1)S(1)} %copy-done.1), channel_id=1, source_target_pairs={{0,2},{1,3},{2,0},{3,1},{4,6},{5,7},{6,4},{7,5},{8,10},{9,11},{10,... | collective-permute-start | bytes 3145736 | tf_op jit(solution)/shard_map/ppermute | solution.py:331
  81.8 40.9 %collective-permute-start.25 = (bf16[1,2048,256]{2,1,0:T(8,128)(2,1)S(1)}, bf16[1,2048,256]{2,1,0:T(8,128)(2,1)S(1)}, u32[]{:S(2)}, u32[]{:S(2)}) collective-permute-start(bf16[1,2048,256]{2,1,0:T(8,128)(2,1)S(1)} %collective-permute-done.24), channel_id=1, source_target_pairs={{0,1},{1,0},{2,3},{3,2},{4,5},{5,4},{6,7},{7,6},{8,9},{9,8},{10,11... | collective-permute-start | bytes 3145736 | tf_op jit(solution)/shard_map/ppermute | solution.py:333
  81.8 41.6 %collective-permute-start.22 = (bf16[1,2048,256]{2,1,0:T(8,128)(2,1)S(1)}, bf16[1,2048,256]{2,1,0:T(8,128)(2,1)S(1)}, u32[]{:S(2)}, u32[]{:S(2)}) collective-permute-start(bf16[1,2048,256]{2,1,0:T(8,128)(2,1)S(1)} %collective-permute-done.21), channel_id=1, source_target_pairs={{0,1},{1,0},{2,3},{3,2},{4,5},{5,4},{6,7},{7,6},{8,9},{9,8},{10,11... | collective-permute-start | bytes 3145736 | tf_op jit(solution)/shard_map/ppermute | solution.py:333
  82.3 45.3 %collective-permute-start.26 = (bf16[1,256,2048]{2,1,0:T(8,128)(2,1)S(1)}, bf16[1,256,2048]{2,1,0:T(8,128)(2,1)S(1)}, u32[]{:S(2)}, u32[]{:S(2)}) collective-permute-start(bf16[1,256,2048]{2,1,0:T(8,128)(2,1)S(1)} %copy-done), channel_id=1, source_target_pairs={{0,1},{1,0},{2,3},{3,2},{4,5},{5,4},{6,7},{7,6},{8,9},{9,8},{10,11... | collective-permute-start | bytes 3145736 | tf_op jit(solution)/shard_map/ppermute | solution.py:332
  104.3 23.4 %collective-permute-start.28 = (bf16[1,256,2048]{2,1,0:T(8,128)(2,1)S(1)}, bf16[1,256,2048]{2,1,0:T(8,128)(2,1)S(1)}, u32[]{:S(2)}, u32[]{:S(2)}) collective-permute-start(bf16[1,256,2048]{2,1,0:T(8,128)(2,1)S(1)} %collective-permute-done.27), channel_id=1, source_target_pairs={{0,1},{1,0},{2,3},{3,2},{4,5},{5,4},{6,7},{7,6},{8,9},{9,8},{10,11... | collective-permute-start | bytes 3145736 | tf_op jit(solution)/shard_map/ppermute | solution.py:333
  122.7 31.4 %collective-permute-start.14 = (bf16[256,2048]{1,0:T(8,128)(2,1)S(1)}, bf16[256,2048]{1,0:T(8,128)(2,1)S(1)}, u32[]{:S(2)}, u32[]{:S(2)}) collective-permute-start(bf16[256,2048]{1,0:T(8,128)(2,1)S(1)} %copy-done.1), channel_id=1, source_target_pairs={{0,1},{1,0},{2,3},{3,2},{4,5},{5,4},{6,7},{7,6},{8,9},{9,8},{10,11... | collective-permute-start | bytes 3145736 | tf_op jit(solution)/shard_map/ppermute | solution.py:332
  122.7 32.9 %collective-permute-start.16 = (bf16[256,2048]{1,0:T(8,128)(2,1)S(1)}, bf16[256,2048]{1,0:T(8,128)(2,1)S(1)}, u32[]{:S(2)}, u32[]{:S(2)}) collective-permute-start(bf16[256,2048]{1,0:T(8,128)(2,1)S(1)} %collective-permute-done.15.refs_6_), channel_id=1, source_target_pairs={{0,1},{1,0},{2,3},{3,2},{4,5},{5,4},{6,7},{7,6},{8,9},{9,8},{10,11... | collective-permute-start | bytes 3145736 | tf_op jit(solution)/shard_map/ppermute | solution.py:333
  129.7 14.0 %collective-permute-start.36 = (bf16[64,2048]{1,0:T(8,128)(2,1)S(1)}, bf16[64,2048]{1,0:T(8,128)(2,1)S(1)}, u32[]{:S(2)}, u32[]{:S(2)}) collective-permute-start(bf16[64,2048]{1,0:T(8,128)(2,1)S(1)} %get-tuple-element.65), channel_id=1, source_target_pairs={{0,4},{4,0},{8,12},{12,8},{16,20},{20,16},{24,28},{28,24},{1,5},{5... | collective-permute-start | bytes 786440 | tf_op jit(solution)/shard_map/ppermute | solution.py:564
  131.0 17.1 %collective-permute-start.34 = (bf16[64,2048]{1,0:T(8,128)(2,1)S(1)}, bf16[64,2048]{1,0:T(8,128)(2,1)S(1)}, u32[]{:S(2)}, u32[]{:S(2)}) collective-permute-start(bf16[64,2048]{1,0:T(8,128)(2,1)S(1)} %get-tuple-element.63), channel_id=1, source_target_pairs={{0,4},{4,0},{8,12},{12,8},{16,20},{20,16},{24,28},{28,24},{1,5},{5... | collective-permute-start | bytes 786440 | tf_op jit(solution)/shard_map/ppermute | solution.py:564
  154.0 23.2 %collective-permute-start.37 = (bf16[64,2048]{1,0:T(8,128)(2,1)S(1)}, bf16[64,2048]{1,0:T(8,128)(2,1)S(1)}, u32[]{:S(2)}, u32[]{:S(2)}) collective-permute-start(bf16[64,2048]{1,0:T(8,128)(2,1)S(1)} %shard_map.144), channel_id=1, source_target_pairs={{0,16},{4,20},{8,24},{12,28},{16,0},{20,4},{24,8},{28,12},{1,17},{... | collective-permute-start | bytes 786440 | tf_op jit(solution)/shard_map/ppermute | solution.py:569
  154.1 23.2 %collective-permute-start.35 = (bf16[64,2048]{1,0:T(8,128)(2,1)S(1)}, bf16[64,2048]{1,0:T(8,128)(2,1)S(1)}, u32[]{:S(2)}, u32[]{:S(2)}) collective-permute-start(bf16[64,2048]{1,0:T(8,128)(2,1)S(1)} %shard_map.143), channel_id=1, source_target_pairs={{0,8},{4,12},{8,0},{12,4},{16,24},{20,28},{24,16},{28,20},{1,9},{5... | collective-permute-start | bytes 786440 | tf_op jit(solution)/shard_map/ppermute | solution.py:569
  (28 other events, 267.9 us)

commit v3 on v2

--- a/solution.py
+++ b/solution.py
@@ -21,7 +21,7 @@
 bf16 = jnp.bfloat16
 f32 = jnp.float32
 
-RETURN_ORDER = (2, 3, 1, 0)
+RETURN_ORDER = (2, 4, 1, 3, 0)
 
 VMEM = pl.BlockSpec(memory_space=pltpu.VMEM)
 
@@ -484,15 +484,14 @@
         out_ref[:, i * part : (i + 1) * part] = (gate / (1.0 + jnp.exp(-gate)) * up).astype(bf16)
 
 
-def contract_body(h_ref, d0, d1, d2, d3, *out_refs):
-    cap = out_refs[0].shape[0]
+def contract_body(h_ref, d0, d1, d2, d3, *out_refs, starts):
     part = d0.shape[0]
     total = None
     for i, d in enumerate((d0, d1, d2, d3)):
         got = mm(h_ref[:, i * part : (i + 1) * part], d[...])
         total = got if total is None else total + got
-    for k, ref in enumerate(out_refs):
-        ref[...] = total[k * cap : (k + 1) * cap].astype(bf16)
+    for start, ref in zip(starts, out_refs):
+        ref[...] = total[start : start + ref.shape[0]].astype(bf16)
 
 
 def join_body(own_ref, other_ref, mix_ref, out_ref, *, first):
@@ -507,11 +506,8 @@
 
 def restore_body(turn_ref, *refs):
     out_ref = refs[-1]
-    cap = refs[0].shape[0]
-    total = None
-    for k, ref in enumerate(refs[:-1]):
-        got = mm(turn_ref[:, k * cap : (k + 1) * cap], ref[...])
-        total = got if total is None else total + got
+    rows = jnp.concatenate([ref[...] for ref in refs[:-1]], axis=0)
+    total = mm(turn_ref[...], rows)
     out_ref[...] = total.astype(bf16)
 
 
@@ -525,7 +521,6 @@
 
     across = [(i, i ^ 1) for i in range(ep_count)]
     row_type = jax.ShapeDtypeStruct((cap, width + LANES), bf16)
-    wide_type = jax.ShapeDtypeStruct((cap, width), bf16)
     route_args = (moe_input, moe_gain.reshape(1, width), expert_pick.T, route_weight.T)
     *sent, turn = call(
         functools.partial(route_body, cap=cap),
@@ -541,8 +536,11 @@
     ups = [u[0] for u in ups]
     piece_type = jax.ShapeDtypeStruct(gates[0].shape, bf16)
     gates[0], ups[0] = call(stage_body, [piece_type] * 2, [VMEM] * 2, 8)(gates[0], ups[0])
+    half = cap // 2
+    pieces = [(0, 0, cap), (1, 0, cap), (2, 0, half), (3, 0, cap), (2, half, half)]
+    starts = [k * cap + first for k, first, _ in pieces]
     results = {}
-    for side, rows in (("a", own), ("b", theirs)):
+    for side, arrived in (("a", own), ("b", theirs)):
         hidden, got = call(
             expand_body,
             [
@@ -552,24 +550,32 @@
             [VMEM] * (GROUPS + 8),
             16,
             flops=4 * count * width * 4 * part,
-        )(*rows, *gates, *ups)
+        )(*arrived, *gates, *ups)
         if side == "a":
             mix = got
         results[side] = call(
-            contract_body, [wide_type] * GROUPS, [VMEM] * 5, 16, flops=2 * count * width * 4 * part
+            functools.partial(contract_body, starts=starts),
+            [jax.ShapeDtypeStruct((rows, width), bf16) for _, _, rows in pieces],
+            [VMEM] * 5,
+            16,
+            flops=2 * count * width * 4 * part,
         )(hidden, *[d[0] for d in downs])
-    others = [None] * GROUPS
-    returned = [None] * GROUPS
-    for k in RETURN_ORDER:
-        others[k] = lax.ppermute(results["b"][k], "ep", across)
-    for k in RETURN_ORDER:
+    others, returned = {}, {}
+    for i in RETURN_ORDER:
+        others[i] = lax.ppermute(results["b"][i], "ep", across)
+    for i in RETURN_ORDER:
+        k, _, rows = pieces[i]
         joined = call(
-            functools.partial(join_body, first=k * cap), wide_type, [VMEM] * 3, 4
-        )(results["a"][k], others[k], mix)
-        returned[k] = lax.ppermute(joined, "ep", along(k)) if k else joined
+            functools.partial(join_body, first=starts[i]),
+            jax.ShapeDtypeStruct((rows, width), bf16),
+            [VMEM] * 3,
+            4,
+        )(results["a"][i], others[i], mix)
+        returned[i] = lax.ppermute(joined, "ep", along(k)) if k else joined
+    order = sorted(range(len(pieces)), key=lambda i: starts[i])
     return call(
-        restore_body, jax.ShapeDtypeStruct((tokens, width), bf16), [VMEM] * (GROUPS + 1), 8
-    )(turn, *returned)
+        restore_body, jax.ShapeDtypeStruct((tokens, width), bf16), [VMEM] * (len(pieces) + 1), 8
+    )(turn, *[returned[i] for i in order])
 
 
 def expand(arrived, gate_weights, up_weights):

time: 179 us -> 200 us (1.12)
  waiting for transfers between devices: 94.9 us -> 117 us
  local copies, waits for them, and re-layouts: 6.88 us -> 4.43 us
    ppermute x4, waiting for transfers between devices: 47 us -> 76.6 us  [spread(): far = lax.ppermute(piece, 'tp', cross)]
    ppermute x7 -> x9, waiting for transfers between devices: 32.3 us -> 23.7 us  [the longest x4 16.4 us: paired_experts(): returned[i] = lax.ppermute(joined, 'ep', along(k)) if k else joined]
    ppermute x3, starting transfers between devices: 6.99 us -> 4.45 us  [mixer(): attended[k] = lax.ppermute(attended[k], 'ep', pairs)]
    unnamed x24, local copies, waits for them, and re-layouts: 6.88 us -> 4.43 us
    ppermute x3, waiting for transfers between devices: 3.07 us -> 0.86 us  [mixer(): attended[k] = lax.ppermute(attended[k], 'ep', pairs)]
    ppermute x7 -> x9, starting transfers between devices: 8.1 us -> 8.98 us  [the longest x4 4.65 us: paired_experts(): returned[i] = lax.ppermute(joined, 'ep', along(k)) if k else joined]
  transfers between devices with their start and end apart: 40 -> 42, of which waited for: 13 -> 14; matrix products, arithmetic and copies ran while one was open for 0% -> 0% of each run, Pallas kernels for 16% -> 15%
where the time goes in v3:
time: 200 us; the launch traced here: 199 us
  waiting for transfers between devices  117 us (58%)
  starting transfers between devices  46.3 us (23%)
  Pallas kernels  31 us (16%)
  local copies, waits for them, and re-layouts  4.43 us (2%)
    ppermute x4, waiting for transfers between devices, spread(): far = lax.ppermute(piece, 'tp', cross)  76.6 us
    pallas_call x1, Pallas kernels, mixer(): call(functools.partial(attend_pair_body, **sizes), [jax.ShapeDtypeStruct(...  18 us
    ppermute x4, waiting for transfers between devices, paired_experts(): returned[i] = lax.ppermute(joined, 'ep', along(k)) if k else joined  16.4 us
    ppermute x3, waiting for transfers between devices, mixer(): own.append(lax.ppermute(packed[k], 'ep', pairs))  8.73 us
    ppermute x5, waiting for transfers between devices, paired_experts(): others[i] = lax.ppermute(results['b'][i], 'ep', across)  7.25 us
    ppermute x3, starting transfers between devices, paired_experts(): lax.ppermute(sent[k], 'ep', along(k))  6.21 us
    ppermute x4, starting transfers between devices, spread(): far = lax.ppermute(piece, 'tp', cross)  5.95 us
    ppermute x3, starting transfers between devices, mixer(): own.append(lax.ppermute(packed[k], 'ep', pairs))  5.71 us
  transfers between devices with their start and end apart: 42, of which 14 were waited for; matrix products, arithmetic and copies ran while one was open for 0% of the time, Pallas kernels for 15%

profile of v3, /device:TPU:0, one launch (start us, length us, event | category | flops | bytes accessed | tf_op | source)
XLA Modules:
  0.0 199.3 jit_solution(18414328569817855619)
XLA Ops:
  4.7 3.1 %collective-permute-start = (bf16[768,128]{1,0:T(8,128)(2,1)S(1)}, bf16[768,128]{1,0:T(8,128)(2,1)S(1)}, u32[]{:S(2)}, u32[]{:S(2)}) collective-permute-start(bf16[768,128]{1,0:T(8,128)(2,1)S(1)} %get-tuple-element.39), channel_id=1, source_target_pairs={{0,8},{4,12},{8,0},{12,4},{16,24},{20,28},{24,16},{28,20},{1,9},{5... | collective-permute-start | bytes 589832 | tf_op jit(solution)/shard_map/ppermute | solution.py:370
  7.9 2.6 %collective-permute-start.1 = (bf16[768,128]{1,0:T(8,128)(2,1)S(1)}, bf16[768,128]{1,0:T(8,128)(2,1)S(1)}, u32[]{:S(2)}, u32[]{:S(2)}) collective-permute-start(bf16[768,128]{1,0:T(8,128)(2,1)S(1)} %get-tuple-element.40), channel_id=1, source_target_pairs={{0,16},{4,20},{8,24},{12,28},{16,0},{20,4},{24,8},{28,12},{1,17},{... | collective-permute-start | bytes 589832 | tf_op jit(solution)/shard_map/ppermute | solution.py:370
  14.3 2.8 %collective-permute-done.refs_1_ = bf16[768,128]{1,0:T(8,128)(2,1)S(1)} collective-permute-done((bf16[768,128]{1,0:T(8,128)(2,1)S(1)}, bf16[768,128]{1,0:T(8,128)(2,1)S(1)}, u32[]{:S(2)}, u32[]{:S(2)}) %collective-permute-start) | collective-permute-done | bytes 196640 | tf_op jit(solution)/shard_map/ppermute | solution.py:370
  17.1 2.0 collective-permute-start.4
  19.0 6.0 %collective-permute-done.1.refs_2_ = bf16[768,128]{1,0:T(8,128)(2,1)S(1)} collective-permute-done((bf16[768,128]{1,0:T(8,128)(2,1)S(1)}, bf16[768,128]{1,0:T(8,128)(2,1)S(1)}, u32[]{:S(2)}, u32[]{:S(2)}) %collective-permute-start.1) | collective-permute-done | bytes 196640 | tf_op jit(solution)/shard_map/ppermute | solution.py:370
  27.0 3.9 %collective-permute-start.18 = (bf16[64,2176]{1,0:T(8,128)(2,1)S(1)}, bf16[64,2176]{1,0:T(8,128)(2,1)S(1)}, u32[]{:S(2)}, u32[]{:S(2)}) collective-permute-start(bf16[64,2176]{1,0:T(8,128)(2,1)S(1)} %get-tuple-element.55), channel_id=1, source_target_pairs={{0,16},{4,20},{8,24},{12,28},{16,0},{20,4},{24,8},{28,12},{1,17},{... | collective-permute-start | bytes 835592 | tf_op jit(solution)/shard_map/ppermute | solution.py:531
  32.3 2.4 %collective-permute-start.29 = (bf16[64,2176]{1,0:T(8,128)(2,1)S(1)}, bf16[64,2176]{1,0:T(8,128)(2,1)S(1)}, u32[]{:S(2)}, u32[]{:S(2)}) collective-permute-start(bf16[64,2176]{1,0:T(8,128)(2,1)S(1)} %get-tuple-element.53.refs_0_), channel_id=1, source_target_pairs={{0,4},{4,0},{8,12},{12,8},{16,20},{20,16},{24,28},{28,24},{1,5},{5... | collective-permute-start | bytes 835592 | tf_op jit(solution)/shard_map/ppermute | solution.py:532
  34.8 18.0 %shard_map.132 = (bf16[2,4,32,128]{3,2,1,0:T(8,128)(2,1)S(1)}, bf16[2,4,32,128]{3,2,1,0:T(8,128)(2,1)S(1)}, bf16[2,4,32,128]{3,2,1,0:T(8,128)(2,1)S(1)}, bf16[2,4,32,128]{3,2,1,0:T(8,128)(2,1)S(1)}) custom-call(f32[16,256]{1,0:T(8,128)S(1)} %get-tuple-element.37.bias_ref, bf16[768,128]{1,0:T(8,128)(2,1)S(1)} %get-tuple-element.38.refs_0_, ...), custom_call_target="tpu_custom_call" | custom-call | flops 3221225472 | tf_op jit(solution)/shard_map/pallas_call | solution.py:374
  55.4 1.8 collective-permute-start.9
  57.2 2.0 collective-permute-start.31
  63.1 1.7 collective-permute-done.31.refs_2_
  64.8 3.0 %collective-permute-done.32.refs_3_ = bf16[64,2176]{1,0:T(8,128)(2,1)S(1)} collective-permute-done((bf16[64,2176]{1,0:T(8,128)(2,1)S(1)}, bf16[64,2176]{1,0:T(8,128)(2,1)S(1)}, u32[]{:S(2)}, u32[]{:S(2)}) %collective-permute-start.32) | collective-permute-done | bytes 278560 | tf_op jit(solution)/shard_map/ppermute | solution.py:532
  69.3 16.8 %collective-permute-done.24 = bf16[1,2048,256]{2,1,0:T(8,128)(2,1)S(1)} collective-permute-done((bf16[1,2048,256]{2,1,0:T(8,128)(2,1)S(1)}, bf16[1,2048,256]{2,1,0:T(8,128)(2,1)S(1)}, u32[]{:S(2)}, u32[]{:S(2)}) %collective-permute-start.24) | collective-permute-done | bytes 1048608 | tf_op jit(solution)/shard_map/ppermute | solution.py:331
  87.6 21.0 %collective-permute-done.21 = bf16[1,2048,256]{2,1,0:T(8,128)(2,1)S(1)} collective-permute-done((bf16[1,2048,256]{2,1,0:T(8,128)(2,1)S(1)}, bf16[1,2048,256]{2,1,0:T(8,128)(2,1)S(1)}, u32[]{:S(2)}, u32[]{:S(2)}) %collective-permute-start.21) | collective-permute-done | bytes 1048608 | tf_op jit(solution)/shard_map/ppermute | solution.py:331
  109.2 21.9 %collective-permute-done.27 = bf16[1,256,2048]{2,1,0:T(8,128)(2,1)S(1)} collective-permute-done((bf16[1,256,2048]{2,1,0:T(8,128)(2,1)S(1)}, bf16[1,256,2048]{2,1,0:T(8,128)(2,1)S(1)}, u32[]{:S(2)}, u32[]{:S(2)}) %collective-permute-start.27) | collective-permute-done | bytes 1048608 | tf_op jit(solution)/shard_map/ppermute | solution.py:331
  131.1 16.9 %collective-permute-done.15.refs_6_ = bf16[256,2048]{1,0:T(8,128)(2,1)S(1)} collective-permute-done((bf16[256,2048]{1,0:T(8,128)(2,1)S(1)}, bf16[256,2048]{1,0:T(8,128)(2,1)S(1)}, u32[]{:S(2)}, u32[]{:S(2)}) %collective-permute-start.15) | collective-permute-done | bytes 1048608 | tf_op jit(solution)/shard_map/ppermute | solution.py:331
  150.1 2.9 %shard_map.140 = (bf16[256,1024]{1,0:T(8,128)(2,1)S(1)}, bf16[256,128]{1,0:T(8,128)(2,1)}) custom-call(bf16[64,2176]{1,0:T(8,128)(2,1)S(1)} %collective-permute-done.29.refs_0_, bf16[64,2176]{1,0:T(8,128)(2,1)S(1)} %collective-permute-done.30.refs_1_, bf16[64,2176]{1,0:T(8,128)(2,1)S(1)} %collective-permute-done.31.refs_2_, ...), custom_call_target="tpu_custom_call" | custom-call | flops 2147483648 | tf_op jit(solution)/shard_map/pallas_call | solution.py:544
  157.6 2.0 %collective-permute-done.12.refs_2_ = bf16[8,32,128]{2,1,0:T(8,128)(2,1)S(1)} collective-permute-done((bf16[8,32,128]{2,1,0:T(8,128)(2,1)S(1)}, bf16[8,32,128]{2,1,0:T(8,128)(2,1)S(1)}, u32[]{:S(2)}, u32[]{:S(2)}) %collective-permute-start.12) | collective-permute-done | bytes 65568 | tf_op jit(solution)/shard_map/ppermute | solution.py:398
  163.0 2.4 %shard_map.138 = (bf16[256,1024]{1,0:T(8,128)(2,1)S(1)}, bf16[256,128]{1,0:T(8,128)(2,1)S(1)}) custom-call(bf16[64,2176]{1,0:T(8,128)(2,1)S(1)} %get-tuple-element.53.refs_0_, bf16[64,2176]{1,0:T(8,128)(2,1)S(1)} %collective-permute-done.17.refs_1_, bf16[64,2176]{1,0:T(8,128)(2,1)S(1)} %collective-permute-done.18.refs_2_, ...), custom_call_target="tpu_custom_call" | custom-call | flops 2147483648 | tf_op jit(solution)/shard_map/pallas_call | solution.py:544
  166.9 6.6 %collective-permute-done.34.other_ref = bf16[64,2048]{1,0:T(8,128)(2,1)S(1)} collective-permute-done((bf16[64,2048]{1,0:T(8,128)(2,1)S(1)}, bf16[64,2048]{1,0:T(8,128)(2,1)S(1)}, u32[]{:S(2)}, u32[]{:S(2)}) %collective-permute-start.34) | collective-permute-done | bytes 262176 | tf_op jit(solution)/shard_map/ppermute | solution.py:565
  174.7 1.7 collective-permute-start.41
  176.9 2.9 %collective-permute-start.39 = (bf16[32,2048]{1,0:T(8,128)(2,1)S(1)}, bf16[32,2048]{1,0:T(8,128)(2,1)S(1)}, u32[]{:S(2)}, u32[]{:S(2)}) collective-permute-start(bf16[32,2048]{1,0:T(8,128)(2,1)S(1)} %shard_map.145), channel_id=1, source_target_pairs={{0,16},{4,20},{8,24},{12,28},{16,0},{20,4},{24,8},{28,12},{1,17},{... | collective-permute-start | bytes 393224 | tf_op jit(solution)/shard_map/ppermute | solution.py:574
  179.8 1.6 shard_map.135
  181.7 15.0 %collective-permute-done.39.refs_3_ = bf16[32,2048]{1,0:T(8,128)(2,1)S(1)} collective-permute-done((bf16[32,2048]{1,0:T(8,128)(2,1)S(1)}, bf16[32,2048]{1,0:T(8,128)(2,1)S(1)}, u32[]{:S(2)}, u32[]{:S(2)}) %collective-permute-start.39) | collective-permute-done | bytes 131104 | tf_op jit(solution)/shard_map/ppermute | solution.py:574
  (101 shorter events, 37.7 us)
Async XLA Ops:
  7.9 17.1 %collective-permute-start.1 = (bf16[768,128]{1,0:T(8,128)(2,1)S(1)}, bf16[768,128]{1,0:T(8,128)(2,1)S(1)}, u32[]{:S(2)}, u32[]{:S(2)}) collective-permute-start(bf16[768,128]{1,0:T(8,128)(2,1)S(1)} %get-tuple-element.40), channel_id=1, source_target_pairs={{0,16},{4,20},{8,24},{12,28},{16,0},{20,4},{24,8},{28,12},{1,17},{... | collective-permute-start | bytes 589832 | tf_op jit(solution)/shard_map/ppermute | solution.py:370
  10.4 16.1 %collective-permute-start.2 = (bf16[768,128]{1,0:T(8,128)(2,1)S(1)}, bf16[768,128]{1,0:T(8,128)(2,1)S(1)}, u32[]{:S(2)}, u32[]{:S(2)}) collective-permute-start(bf16[768,128]{1,0:T(8,128)(2,1)S(1)} %get-tuple-element.41), channel_id=1, source_target_pairs={{0,24},{4,28},{8,16},{12,20},{16,8},{20,12},{24,0},{28,4},{1,25},{... | collective-permute-start | bytes 589832 | tf_op jit(solution)/shard_map/ppermute | solution.py:370
  11.8 19.1 %collective-permute-start.17 = (bf16[64,2176]{1,0:T(8,128)(2,1)S(1)}, bf16[64,2176]{1,0:T(8,128)(2,1)S(1)}, u32[]{:S(2)}, u32[]{:S(2)}) collective-permute-start(bf16[64,2176]{1,0:T(8,128)(2,1)S(1)} %get-tuple-element.54), channel_id=1, source_target_pairs={{0,8},{4,12},{8,0},{12,4},{16,24},{20,28},{24,16},{28,20},{1,9},{5... | collective-permute-start | bytes 835592 | tf_op jit(solution)/shard_map/ppermute | solution.py:531
  27.0 27.2 %collective-permute-start.18 = (bf16[64,2176]{1,0:T(8,128)(2,1)S(1)}, bf16[64,2176]{1,0:T(8,128)(2,1)S(1)}, u32[]{:S(2)}, u32[]{:S(2)}) collective-permute-start(bf16[64,2176]{1,0:T(8,128)(2,1)S(1)} %get-tuple-element.55), channel_id=1, source_target_pairs={{0,16},{4,20},{8,24},{12,28},{16,0},{20,4},{24,8},{28,12},{1,17},{... | collective-permute-start | bytes 835592 | tf_op jit(solution)/shard_map/ppermute | solution.py:531
  31.0 24.5 %collective-permute-start.19 = (bf16[64,2176]{1,0:T(8,128)(2,1)S(1)}, bf16[64,2176]{1,0:T(8,128)(2,1)S(1)}, u32[]{:S(2)}, u32[]{:S(2)}) collective-permute-start(bf16[64,2176]{1,0:T(8,128)(2,1)S(1)} %get-tuple-element.56), channel_id=1, source_target_pairs={{0,24},{4,28},{8,16},{12,20},{16,8},{20,12},{24,0},{28,4},{1,25},{... | collective-permute-start | bytes 835592 | tf_op jit(solution)/shard_map/ppermute | solution.py:531
  32.3 24.9 %collective-permute-start.29 = (bf16[64,2176]{1,0:T(8,128)(2,1)S(1)}, bf16[64,2176]{1,0:T(8,128)(2,1)S(1)}, u32[]{:S(2)}, u32[]{:S(2)}) collective-permute-start(bf16[64,2176]{1,0:T(8,128)(2,1)S(1)} %get-tuple-element.53.refs_0_), channel_id=1, source_target_pairs={{0,4},{4,0},{8,12},{12,8},{16,20},{20,16},{24,28},{28,24},{1,5},{5... | collective-permute-start | bytes 835592 | tf_op jit(solution)/shard_map/ppermute | solution.py:532
  34.7 28.4 %collective-permute-start.30 = (bf16[64,2176]{1,0:T(8,128)(2,1)S(1)}, bf16[64,2176]{1,0:T(8,128)(2,1)S(1)}, u32[]{:S(2)}, u32[]{:S(2)}) collective-permute-start(bf16[64,2176]{1,0:T(8,128)(2,1)S(1)} %collective-permute-done.17.refs_1_), channel_id=1, source_target_pairs={{0,4},{4,0},{8,12},{12,8},{16,20},{20,16},{24,28},{28,24},{1,5},{5... | collective-permute-start | bytes 835592 | tf_op jit(solution)/shard_map/ppermute | solution.py:532
  60.1 26.0 %collective-permute-start.24 = (bf16[1,2048,256]{2,1,0:T(8,128)(2,1)S(1)}, bf16[1,2048,256]{2,1,0:T(8,128)(2,1)S(1)}, u32[]{:S(2)}, u32[]{:S(2)}) collective-permute-start(bf16[1,2048,256]{2,1,0:T(8,128)(2,1)S(1)} %copy-done.3), channel_id=1, source_target_pairs={{0,2},{1,3},{2,0},{3,1},{4,6},{5,7},{6,4},{7,5},{8,10},{9,11},{10,... | collective-permute-start | bytes 3145736 | tf_op jit(solution)/shard_map/ppermute | solution.py:331
  61.6 47.0 %collective-permute-start.21 = (bf16[1,2048,256]{2,1,0:T(8,128)(2,1)S(1)}, bf16[1,2048,256]{2,1,0:T(8,128)(2,1)S(1)}, u32[]{:S(2)}, u32[]{:S(2)}) collective-permute-start(bf16[1,2048,256]{2,1,0:T(8,128)(2,1)S(1)} %copy-done.2), channel_id=1, source_target_pairs={{0,2},{1,3},{2,0},{3,1},{4,6},{5,7},{6,4},{7,5},{8,10},{9,11},{10,... | collective-permute-start | bytes 3145736 | tf_op jit(solution)/shard_map/ppermute | solution.py:331
  63.1 45.5 %collective-permute-start.20 = (bf16[1,2048,256]{2,1,0:T(8,128)(2,1)S(1)}, bf16[1,2048,256]{2,1,0:T(8,128)(2,1)S(1)}, u32[]{:S(2)}, u32[]{:S(2)}) collective-permute-start(bf16[1,2048,256]{2,1,0:T(8,128)(2,1)S(1)} %copy-done.2), channel_id=1, source_target_pairs={{0,1},{1,0},{2,3},{3,2},{4,5},{5,4},{6,7},{7,6},{8,9},{9,8},{10,11... | collective-permute-start | bytes 3145736 | tf_op jit(solution)/shard_map/ppermute | solution.py:332
  64.8 44.3 %collective-permute-start.23 = (bf16[1,2048,256]{2,1,0:T(8,128)(2,1)S(1)}, bf16[1,2048,256]{2,1,0:T(8,128)(2,1)S(1)}, u32[]{:S(2)}, u32[]{:S(2)}) collective-permute-start(bf16[1,2048,256]{2,1,0:T(8,128)(2,1)S(1)} %copy-done.3), channel_id=1, source_target_pairs={{0,1},{1,0},{2,3},{3,2},{4,5},{5,4},{6,7},{7,6},{8,9},{9,8},{10,11... | collective-permute-start | bytes 3145736 | tf_op jit(solution)/shard_map/ppermute | solution.py:332
  67.8 63.3 %collective-permute-start.27 = (bf16[1,256,2048]{2,1,0:T(8,128)(2,1)S(1)}, bf16[1,256,2048]{2,1,0:T(8,128)(2,1)S(1)}, u32[]{:S(2)}, u32[]{:S(2)}) collective-permute-start(bf16[1,256,2048]{2,1,0:T(8,128)(2,1)S(1)} %copy-done), channel_id=1, source_target_pairs={{0,2},{1,3},{2,0},{3,1},{4,6},{5,7},{6,4},{7,5},{8,10},{9,11},{10,... | collective-permute-start | bytes 3145736 | tf_op jit(solution)/shard_map/ppermute | solution.py:331
  86.1 61.8 %collective-permute-start.15 = (bf16[256,2048]{1,0:T(8,128)(2,1)S(1)}, bf16[256,2048]{1,0:T(8,128)(2,1)S(1)}, u32[]{:S(2)}, u32[]{:S(2)}) collective-permute-start(bf16[256,2048]{1,0:T(8,128)(2,1)S(1)} %copy-done.1), channel_id=1, source_target_pairs={{0,2},{1,3},{2,0},{3,1},{4,6},{5,7},{6,4},{7,5},{8,10},{9,11},{10,... | collective-permute-start | bytes 3145736 | tf_op jit(solution)/shard_map/ppermute | solution.py:331
  108.6 39.4 %collective-permute-start.25 = (bf16[1,2048,256]{2,1,0:T(8,128)(2,1)S(1)}, bf16[1,2048,256]{2,1,0:T(8,128)(2,1)S(1)}, u32[]{:S(2)}, u32[]{:S(2)}) collective-permute-start(bf16[1,2048,256]{2,1,0:T(8,128)(2,1)S(1)} %collective-permute-done.24), channel_id=1, source_target_pairs={{0,1},{1,0},{2,3},{3,2},{4,5},{5,4},{6,7},{7,6},{8,9},{9,8},{10,11... | collective-permute-start | bytes 3145736 | tf_op jit(solution)/shard_map/ppermute | solution.py:333
  108.6 40.1 %collective-permute-start.22 = (bf16[1,2048,256]{2,1,0:T(8,128)(2,1)S(1)}, bf16[1,2048,256]{2,1,0:T(8,128)(2,1)S(1)}, u32[]{:S(2)}, u32[]{:S(2)}) collective-permute-start(bf16[1,2048,256]{2,1,0:T(8,128)(2,1)S(1)} %collective-permute-done.21), channel_id=1, source_target_pairs={{0,1},{1,0},{2,3},{3,2},{4,5},{5,4},{6,7},{7,6},{8,9},{9,8},{10,11... | collective-permute-start | bytes 3145736 | tf_op jit(solution)/shard_map/ppermute | solution.py:333
  109.1 43.9 %collective-permute-start.26 = (bf16[1,256,2048]{2,1,0:T(8,128)(2,1)S(1)}, bf16[1,256,2048]{2,1,0:T(8,128)(2,1)S(1)}, u32[]{:S(2)}, u32[]{:S(2)}) collective-permute-start(bf16[1,256,2048]{2,1,0:T(8,128)(2,1)S(1)} %copy-done), channel_id=1, source_target_pairs={{0,1},{1,0},{2,3},{3,2},{4,5},{5,4},{6,7},{7,6},{8,9},{9,8},{10,11... | collective-permute-start | bytes 3145736 | tf_op jit(solution)/shard_map/ppermute | solution.py:332
  131.1 21.9 %collective-permute-start.28 = (bf16[1,256,2048]{2,1,0:T(8,128)(2,1)S(1)}, bf16[1,256,2048]{2,1,0:T(8,128)(2,1)S(1)}, u32[]{:S(2)}, u32[]{:S(2)}) collective-permute-start(bf16[1,256,2048]{2,1,0:T(8,128)(2,1)S(1)} %collective-permute-done.27), channel_id=1, source_target_pairs={{0,1},{1,0},{2,3},{3,2},{4,5},{5,4},{6,7},{7,6},{8,9},{9,8},{10,11... | collective-permute-start | bytes 3145736 | tf_op jit(solution)/shard_map/ppermute | solution.py:333
  148.0 28.9 %collective-permute-start.14 = (bf16[256,2048]{1,0:T(8,128)(2,1)S(1)}, bf16[256,2048]{1,0:T(8,128)(2,1)S(1)}, u32[]{:S(2)}, u32[]{:S(2)}) collective-permute-start(bf16[256,2048]{1,0:T(8,128)(2,1)S(1)} %copy-done.1), channel_id=1, source_target_pairs={{0,1},{1,0},{2,3},{3,2},{4,5},{5,4},{6,7},{7,6},{8,9},{9,8},{10,11... | collective-permute-start | bytes 3145736 | tf_op jit(solution)/shard_map/ppermute | solution.py:332
  148.0 31.7 %collective-permute-start.16 = (bf16[256,2048]{1,0:T(8,128)(2,1)S(1)}, bf16[256,2048]{1,0:T(8,128)(2,1)S(1)}, u32[]{:S(2)}, u32[]{:S(2)}) collective-permute-start(bf16[256,2048]{1,0:T(8,128)(2,1)S(1)} %collective-permute-done.15.refs_6_), channel_id=1, source_target_pairs={{0,1},{1,0},{2,3},{3,2},{4,5},{5,4},{6,7},{7,6},{8,9},{9,8},{10,11... | collective-permute-start | bytes 3145736 | tf_op jit(solution)/shard_map/ppermute | solution.py:333
  160.9 15.4 %collective-permute-start.36 = (bf16[32,2048]{1,0:T(8,128)(2,1)S(1)}, bf16[32,2048]{1,0:T(8,128)(2,1)S(1)}, u32[]{:S(2)}, u32[]{:S(2)}) collective-permute-start(bf16[32,2048]{1,0:T(8,128)(2,1)S(1)} %get-tuple-element.67), channel_id=1, source_target_pairs={{0,4},{4,0},{8,12},{12,8},{16,20},{20,16},{24,28},{28,24},{1,5},{5... | collective-permute-start | bytes 393224 | tf_op jit(solution)/shard_map/ppermute | solution.py:565
  174.7 23.5 %collective-permute-start.41 = (bf16[64,2048]{1,0:T(8,128)(2,1)S(1)}, bf16[64,2048]{1,0:T(8,128)(2,1)S(1)}, u32[]{:S(2)}, u32[]{:S(2)}) collective-permute-start(bf16[64,2048]{1,0:T(8,128)(2,1)S(1)} %shard_map.146), channel_id=1, source_target_pairs={{0,24},{4,28},{8,16},{12,20},{16,8},{20,12},{24,0},{28,4},{1,25},{... | collective-permute-start | bytes 786440 | tf_op jit(solution)/shard_map/ppermute | solution.py:574
  176.3 21.8 %collective-permute-start.35 = (bf16[64,2048]{1,0:T(8,128)(2,1)S(1)}, bf16[64,2048]{1,0:T(8,128)(2,1)S(1)}, u32[]{:S(2)}, u32[]{:S(2)}) collective-permute-start(bf16[64,2048]{1,0:T(8,128)(2,1)S(1)} %shard_map.143), channel_id=1, source_target_pairs={{0,8},{4,12},{8,0},{12,4},{16,24},{20,28},{24,16},{28,20},{1,9},{5... | collective-permute-start | bytes 786440 | tf_op jit(solution)/shard_map/ppermute | solution.py:574
  176.9 19.9 %collective-permute-start.39 = (bf16[32,2048]{1,0:T(8,128)(2,1)S(1)}, bf16[32,2048]{1,0:T(8,128)(2,1)S(1)}, u32[]{:S(2)}, u32[]{:S(2)}) collective-permute-start(bf16[32,2048]{1,0:T(8,128)(2,1)S(1)} %shard_map.145), channel_id=1, source_target_pairs={{0,16},{4,20},{8,24},{12,28},{16,0},{20,4},{24,8},{28,12},{1,17},{... | collective-permute-start | bytes 393224 | tf_op jit(solution)/shard_map/ppermute | solution.py:574
  179.7 18.4 %collective-permute-start.37 = (bf16[32,2048]{1,0:T(8,128)(2,1)S(1)}, bf16[32,2048]{1,0:T(8,128)(2,1)S(1)}, u32[]{:S(2)}, u32[]{:S(2)}) collective-permute-start(bf16[32,2048]{1,0:T(8,128)(2,1)S(1)} %shard_map.144), channel_id=1, source_target_pairs={{0,16},{4,20},{8,24},{12,28},{16,0},{20,4},{24,8},{28,12},{1,17},{... | collective-permute-start | bytes 393224 | tf_op jit(solution)/shard_map/ppermute | solution.py:574
  (30 other events, 315.7 us)
